TPU v7x, 32 devices: a whole 2x2x4 slice. The times are simulated.
32 devices in a mesh: sp: 8 (over z, y), tp: 4 (over x, core).
Axes of the slice: x: 2, y: 2, z: 4, core: 2. Of those that a mesh axis runs over, the one named last changes fastest.
Arguments:
- tokens: bfloat16 [6144, 2048], P(('sp', 'tp')), may hold values from -6 to 6
- norm_gain: float32 [2048], replicated, may hold values from 0.1 to 1.9
- w_query: bfloat16 [2048, 1024], P('sp', 'tp'), may hold values from -0.125 to 0.125
- w_forget: bfloat16 [2048, 1024], P('sp', 'tp'), may hold values from -0.125 to 0.125
- w_input: bfloat16 [2048, 1024], P('sp', 'tp'), may hold values from -0.125 to 0.125
- w_outgate: bfloat16 [2048, 1024], P('sp', 'tp'), may hold values from -0.125 to 0.125
- w_conv_value: bfloat16 [2048, 1024], P('sp', 'tp'), may hold values from -0.125 to 0.125
- w_conv_gate: bfloat16 [2048, 1024], P('sp', 'tp'), may hold values from -0.125 to 0.125
- w_gate_rec: bfloat16 [2048, 2048], P('sp', 'tp'), may hold values from -0.125 to 0.125
- w_gate_conv: bfloat16 [2048, 2048], P('sp', 'tp'), may hold values from -0.125 to 0.125
- lower_bound: float32 [1024], P('tp'), may hold values from 0.92 to 0.99991862, as said below
- decay_shift: float32 [6144, 1024], P('sp', 'tp'), may hold values from -0.7 to 0, as said below
- state_init: float32 [8, 128, 128], P('tp'), may hold values from -0.1875 to 0.1875
- head_gain: float32 [1024], P('tp'), may hold values from 0.1 to 1.9
- conv_kernel: float32 [31, 1024], P(None, 'tp'), may hold values from -7.5 to 7.5
- channel_gain: float32 [1024], P('tp'), may hold values from 0.1 to 1.9
- channel_bias: float32 [1024], P('tp'), may hold values from -3 to 3
- w_out_rec: bfloat16 [1024, 2048], P('tp', 'sp'), may hold values from -0.1875 to 0.1875
- w_out_conv: bfloat16 [1024, 2048], P('tp', 'sp'), may hold values from -0.1875 to 0.1875
Outputs:
- mixed_out: bfloat16 [6144, 2048], P('sp', 'tp')
Inputs may be any that keep to these rules, and one draw needn't show every extreme that they name: `lower_bound`: every entry is below one. `decay_shift`: no entry is positive.
All inputs are finite; a program needn't handle non-finite values.
Results may differ from a plain program's by a relative error of at most 0.017.
Values may be sent and summed in bfloat16 or wider, within the bound.
No kernel may reach another device: no remote copies, remote signals or barrier semaphores. Data moves between devices by JAX's collectives and lax.ppermute only.
A program may use at most 64 MiB of HBM per device.

v0:
```python
import jax
import jax.numpy as jnp
from jax import lax
from jax.sharding import PartitionSpec as P

HEAD = 128
CONV = 1024
KW = 31
BLOCK = 64


EPSILON = 1e-06
highest_precision = lax.Precision.HIGHEST


def prefix(array, axis, combine, identity):
    size, position = (lax.axis_size(axis), lax.axis_index(axis))
    everything = jax.tree.map(
        lambda part, kind: lax.all_gather(part.astype(kind), axis),
        array,
        (jnp.bfloat16, jnp.bfloat16),
    )
    start = jax.tree.map(
        lambda part, zero: jnp.broadcast_to(jnp.asarray(zero, part.dtype), part.shape),
        array,
        identity,
    )

    def lap(k, before):
        reached = k < position
        new = combine(
            before, jax.tree.map(lambda part, own: part[k].astype(own.dtype), everything, array)
        )
        return jax.tree.map(lambda a, b: jnp.where(reached, a, b), new, before)

    return lax.fori_loop(0, size, lap, start)


def passed_along(block, axis, distance):
    devices = range(lax.axis_size(axis))
    route = [(i - distance, i) for i in devices if i - distance in devices]
    return lax.ppermute(block, axis, route)


def normalize_rows(values, gain_vector):
    widened = values.astype(jnp.float32)
    scale = lax.rsqrt(jnp.mean(widened * widened, axis=-1, keepdims=True) + EPSILON)
    return (widened * scale * gain_vector).astype(jnp.bfloat16)


def block_step(state, inputs):
    query, input_gate, values, log_decay = inputs
    length = query.shape[1]
    causal_masked = (jnp.arange(length)[:, None] >= jnp.arange(length)[None, :])[None, :, :, None]
    cumulative = jnp.cumsum(log_decay, axis=1)
    spread = cumulative[:, :, None, :] - cumulative[:, None, :, :]
    weight = jnp.where(causal_masked, jnp.exp(jnp.where(causal_masked, spread, 0.0)), 0.0)
    scores = jnp.einsum("htd,hsd,htsd->hts", query, input_gate, weight, precision=highest_precision)
    output = jnp.einsum("hts,hsv->htv", scores, values, precision=highest_precision)
    output = output + jnp.einsum(
        "htd,hdv->htv", query * jnp.exp(cumulative), state, precision=highest_precision
    )
    final = cumulative[:, -1:, :]
    carried = jnp.exp(final[:, 0, :])[:, :, None] * state
    carried = carried + jnp.einsum(
        "hsd,hsv->hdv",
        input_gate * jnp.exp(final - cumulative),
        values,
        precision=highest_precision,
    )
    return (carried, output)


def compose(preceding_segment, later):
    return (preceding_segment[0] * later[0], later[0][..., None] * preceding_segment[1] + later[1])


def local(
    tokens,
    norm_gain,
    w_query,
    w_forget,
    w_input,
    w_outgate,
    w_conv_value,
    w_conv_gate,
    w_gate_rec,
    w_gate_conv,
    lower_bound,
    decay_shift,
    state_init,
    head_gain,
    conv_kernel,
    channel_gain,
    channel_bias,
    w_out_rec,
    w_out_conv,
):
    tp_count = lax.axis_size("tp")
    normed = normalize_rows(lax.all_gather(tokens, "tp", axis=0, tiled=True), norm_gain)
    row_count = normed.shape[0]
    weights = (
        w_query,
        w_forget,
        w_input,
        w_outgate,
        w_conv_value,
        w_conv_gate,
        w_gate_rec,
        w_gate_conv,
    )
    portions = (
        lax.all_gather(weights[0], "sp", axis=0, tiled=True),
        lax.all_gather(weights[1], "sp", axis=0, tiled=True),
        lax.all_gather(weights[2], "sp", axis=0, tiled=True),
        lax.all_gather(weights[3], "sp", axis=0, tiled=True),
        lax.all_gather(weights[4], "sp", axis=0, tiled=True),
        lax.all_gather(weights[5], "sp", axis=0, tiled=True),
        lax.all_gather(weights[6], "sp", axis=0, tiled=True),
        lax.all_gather(weights[7], "sp", axis=0, tiled=True),
    )
    sums = tuple(
        (jnp.dot(normed, portion, preferred_element_type=jnp.float32) for portion in portions)
    )
    (
        query_raw,
        forget_raw,
        input_raw,
        outgate_raw,
        value_raw,
        gate_raw,
        gate_rec_raw,
        gate_conv_raw,
    ) = tuple((overall_aggregate.astype(jnp.bfloat16) for overall_aggregate in sums))
    local_heads = w_query.shape[1] // HEAD
    block_count = row_count // BLOCK
    query = jax.nn.silu(query_raw.astype(jnp.float32))
    input_gate = (1.0 - lower_bound) * jax.nn.sigmoid(-forget_raw.astype(jnp.float32))
    log_decay = jnp.log1p(-input_gate) + decay_shift
    values = input_raw.astype(jnp.float32)

    def to_blocks(array):
        return array.reshape(block_count, BLOCK, local_heads, HEAD).transpose(0, 2, 1, 3)

    zero_state = jnp.zeros((local_heads, HEAD, HEAD), jnp.float32)
    local_state, blocks_out = lax.scan(
        block_step,
        zero_state,
        (to_blocks(query), to_blocks(input_gate), to_blocks(values), to_blocks(log_decay)),
    )
    local_out = blocks_out.transpose(0, 2, 1, 3).reshape(row_count, local_heads, HEAD)
    running = jnp.cumsum(log_decay, axis=0)
    cumulated_forgetting = jnp.exp(running[-1]).reshape(local_heads, HEAD)
    ones_decay = jnp.ones_like(cumulated_forgetting)
    prefix_decay, prefix_state = prefix(
        (cumulated_forgetting, local_state), "sp", compose, (ones_decay, zero_state)
    )
    incoming_state = prefix_decay[:, :, None] * state_init + prefix_state
    decayed_query = (query * jnp.exp(running)).reshape(row_count, local_heads, HEAD)
    head_out = local_out + jnp.einsum(
        "thd,hdv->thv", decayed_query, incoming_state, precision=highest_precision
    )
    head_out = head_out * lax.rsqrt(jnp.mean(head_out * head_out, axis=-1, keepdims=True) + EPSILON)
    head_out = head_out * head_gain.reshape(local_heads, HEAD)
    mixed_rec = (
        head_out.reshape(row_count, local_heads * HEAD)
        * jax.nn.silu(outgate_raw.astype(jnp.float32))
    ).astype(jnp.bfloat16)
    gated = (value_raw.astype(jnp.float32) * jax.nn.sigmoid(gate_raw.astype(jnp.float32))).astype(
        jnp.bfloat16
    )
    rim_width = KW - 1
    previous = passed_along(gated[row_count - rim_width :], "sp", 1)
    extended = jnp.concatenate([previous, gated], axis=0).astype(jnp.float32)
    conv_out = jnp.zeros((row_count, gated.shape[1]), jnp.float32)
    for tap_index in range(KW):
        conv_out = conv_out + conv_kernel[tap_index] * extended[tap_index : tap_index + row_count]
    squares = lax.psum(jnp.sum(conv_out * conv_out, axis=1), "tp")
    scale = lax.rsqrt(squares / CONV + EPSILON)[:, None]
    mixed_conv = jax.nn.silu(conv_out * scale * channel_gain + channel_bias).astype(jnp.bfloat16)
    rec_columns, conv_columns = (
        lax.all_gather(w_out_rec, "sp", axis=1, tiled=True),
        lax.all_gather(w_out_conv, "sp", axis=1, tiled=True),
    )
    rec_width = mixed_rec.shape[1]
    rec_whole, conv_whole = (
        lax.all_gather(rec_columns, "tp", axis=0, tiled=True),
        lax.all_gather(conv_columns, "tp", axis=0, tiled=True),
    )
    both = jnp.concatenate([mixed_rec, mixed_conv], axis=1).reshape(
        tp_count, row_count // tp_count, -1
    )
    arrived = lax.all_to_all(both, "tp", split_axis=0, concat_axis=2, tiled=True)
    item_count = arrived.shape[1]
    grouped = arrived.reshape(item_count, tp_count, -1)
    rec_part = grouped[:, :, :rec_width].reshape(item_count, -1)
    conv_part = grouped[:, :, rec_width:].reshape(item_count, -1)
    first = jnp.dot(rec_part, rec_whole, preferred_element_type=jnp.float32).astype(jnp.bfloat16)
    second = jnp.dot(conv_part, conv_whole, preferred_element_type=jnp.float32).astype(jnp.bfloat16)
    projected = jnp.stack([first, second], axis=1)[None]
    returned = lax.all_to_all(projected[0], "tp", split_axis=2, concat_axis=0, tiled=True)
    y_rec = returned[:, 0]
    y_conv = returned[:, 1]
    merged = jax.nn.sigmoid(gate_rec_raw.astype(jnp.float32)) * y_rec.astype(jnp.float32)
    merged = merged + jax.nn.sigmoid(gate_conv_raw.astype(jnp.float32)) * y_conv.astype(jnp.float32)
    return merged.astype(jnp.bfloat16)


def solution(mesh):
    in_specs = (
        P(("sp", "tp"), None),
        P(),
        P("sp", "tp"),
        P("sp", "tp"),
        P("sp", "tp"),
        P("sp", "tp"),
        P("sp", "tp"),
        P("sp", "tp"),
        P("sp", "tp"),
        P("sp", "tp"),
        P("tp"),
        P("sp", "tp"),
        P("tp", None, None),
        P("tp"),
        P(None, "tp"),
        P("tp"),
        P("tp"),
        P("tp", "sp"),
        P("tp", "sp"),
    )
    out_specs = P("sp", "tp")
    return jax.shard_map(local, mesh=mesh, in_specs=in_specs, out_specs=out_specs, check_vma=False)
```

profile of v0, /device:TPU:0, one launch (start us, length us, event | category | flops | bytes accessed | tf_op | source)
XLA Modules:
  0.0 553.2 jit_solution(8562246545925976769)
XLA Ops:
  12.8 38.8 %all-gather.31.cloned.1.call-done = bf16[256,2048]{1,0:T(8,128)(2,1)} async-done(((bf16[256,256]{1,0:T(8,128)(2,1)}), bf16[256,2048]{1,0:T(8,128)(2,1)}) %all-gather.31.cloned.1.call-update) | async-done | bytes 1048592 | tf_op jit(solution)/shard_map/all_gather | solution.py:182
  51.6 40.4 %all-gather.35.cloned.1.call-done = bf16[256,2048]{1,0:T(8,128)(2,1)} async-done(((bf16[256,256]{1,0:T(8,128)(2,1)}), bf16[256,2048]{1,0:T(8,128)(2,1)}) %all-gather.35.cloned.1.call-update) | async-done | bytes 1048592 | tf_op jit(solution)/shard_map/all_gather | solution.py:183
  94.8 26.4 %all-gather.15.cloned.1.call-done = bf16[768,2048]{1,0:T(8,128)(2,1)} async-done(((bf16[192,2048]{1,0:T(8,128)(2,1)}), bf16[768,2048]{1,0:T(8,128)(2,1)}) %all-gather.15.cloned.1.call-update) | async-done | bytes 3145744 | tf_op jit(solution)/shard_map/all_gather | solution.py:100
  126.4 37.0 %all-gather.19.cloned.1.call-done = bf16[2048,256]{1,0:T(8,128)(2,1)} async-done(((bf16[256,256]{1,0:T(8,128)(2,1)}), bf16[2048,256]{1,0:T(8,128)(2,1)}) %all-gather.19.cloned.1.call-update) | async-done | bytes 1048592 | tf_op jit(solution)/shard_map/all_gather | solution.py:114
  167.7 36.7 %all-gather.23.cloned.1.call-done = bf16[2048,256]{1,0:T(8,128)(2,1)} async-done(((bf16[256,256]{1,0:T(8,128)(2,1)}), bf16[2048,256]{1,0:T(8,128)(2,1)}) %all-gather.23.cloned.1.call-update) | async-done | bytes 1048592 | tf_op jit(solution)/shard_map/all_gather | solution.py:113
  208.9 36.6 %all-gather.21.cloned.1.call-done = bf16[2048,256]{1,0:T(8,128)(2,1)} async-done(((bf16[256,256]{1,0:T(8,128)(2,1)}), bf16[2048,256]{1,0:T(8,128)(2,1)}) %all-gather.21.cloned.1.call-update) | async-done | bytes 1048592 | tf_op jit(solution)/shard_map/all_gather | solution.py:115
  245.4 4.1 fusion.40
  255.0 115.7 %while.29 = (s32[]{:T(128)}, f32[2,128,128]{2,1,0:T(8,128)S(1)}, f32[12,2,64,128]{3,2,0,1:T(8,128)}, f32[12,2,64,128]{3,2,1,0:T(8,128)}, f32[12,2,64,128]{3,2,1,...) while((s32[]{:T(128)}, f32[2,128,128]{2,1,0:T(8,128)S(1)}, ...), condition=%wide.region_3.4_spmd.clone, body=%wide.region_1.3_spmd.clone.sunk | while | flops 70430720 | bytes 10207360 | solution.py:146
  257.8 3.5 fusion.121
  267.4 3.5 fusion.121
  277.1 3.5 fusion.121
  286.7 3.5 fusion.121
  296.4 3.5 fusion.121
  306.0 3.5 fusion.121
  315.7 3.5 fusion.121
  325.3 3.5 fusion.121
  334.9 3.5 fusion.121
  344.6 3.5 fusion.121
  354.2 3.5 fusion.121
  370.7 31.6 %all-gather = bf16[16,128,128]{2,1,0:T(8,128)(2,1)S(1)} all-gather(bf16[2,128,128]{2,1,0:T(8,128)(2,1)S(1)} %convert_element_type.138), channel_id=2, replica_groups=mesh['sp'=8,'tp'=4] {'sp'}, dimensions={0}, use_global_device_ids=true | all-gather | bytes 589824 | tf_op jit(solution)/shard_map/all_gather | solution.py:19
  403.5 18.4 %all_gather.54 = bf16[8,2,128]{2,1,0:T(2,128)(2,1)S(1)} all-gather(bf16[1,2,128]{2,1,0:T(2,128)(2,1)S(1)} %bitcast.230), channel_id=1, replica_groups=mesh['sp'=8,'tp'=4] {'sp'}, dimensions={0}, use_global_device_ids=true | all-gather | bytes 4608 | tf_op jit(solution)/shard_map/all_gather | solution.py:19
  427.2 4.2 fusion.37
  443.5 5.7 %psum.7 = f32[768]{0:T(1024)S(1)} all-reduce(f32[768]{0:T(1024)S(1)} %get-tuple-element.228), channel_id=1, replica_groups=mesh['sp'=8,'tp'=4] {'tp'}, use_global_device_ids=true, to_apply=%region_10.11 | all-reduce | flops 768 | bytes 6144 | tf_op jit(solution)/shard_map/psum | solution.py:178
  449.6 14.1 %all_to_all.33 = bf16[4,192,512]{2,1,0:T(8,128)(2,1)S(1)} all-to-all(bf16[4,192,512]{2,1,0:T(8,128)(2,1)S(1)} %bitcast.188), channel_id=1, replica_groups=mesh['sp'=8,'tp'=4] {'tp'}, dimensions={0} | all-to-all | bytes 1572864 | tf_op jit(solution)/shard_map/all_to_all | solution.py:193
  470.6 3.8 copy.86
  474.5 3.8 all-to-all-start.1
  478.3 12.4 %all-gather.39.cloned.1.call-done = bf16[2048,512]{1,0:T(8,128)(2,1)} async-done(((bf16[256,512]{1,0:T(8,128)(2,1)}), bf16[2048,512]{1,0:T(8,128)(2,1)}) %all-gather.39.cloned.1.call-update) | async-done | bytes 2097168 | tf_op jit(solution)/shard_map/all_gather | solution.py:120
  490.7 4.3 convolution_convert_fusion.2
  495.0 8.7 %all-to-all-done.1 = bf16[192,2,2048]{0,1,2:T(2,128)(2,1)S(1)} async-done(((bf16[192,2,2048]{0,1,2:T(2,128)(2,1)}), bf16[192,2,2048]{0,1,2:T(2,128)(2,1)S(1)}, u32[]{:S(2)}, u32[]{:S(2)}) %all-to-all-start.1) | async-done | bytes 1572896 | tf_op jit(solution)/shard_map/all_to_all | solution.py:201
  503.7 3.7 copy.87
  507.4 33.0 %all-gather.17.cloned.1.call-done = bf16[2048,512]{1,0:T(8,128)(2,1)} async-done(((bf16[256,512]{1,0:T(8,128)(2,1)}), bf16[2048,512]{1,0:T(8,128)(2,1)}) %all-gather.17.cloned.1.call-update) | async-done | bytes 2097168 | tf_op jit(solution)/shard_map/all_gather | solution.py:119
  540.5 6.2 %fusion.28 = bf16[768,512]{1,0:T(8,128)(2,1)} fusion(bf16[768,512]{1,0:T(8,128)(2,1)S(1)} %convolution_convert_fusion.2, bf16[768,2048]{1,0:T(8,128)(2,1)} %fusion.24, bf16[2048,512]{1,0:T(8,128)(2,1)} %all-gather.17.cloned.1.call-done, bf16[768,2,512]{2,0,1:T(8,128)(2,1)} %bitcast.190), kind=kOutput, calls=%fused_computation.47 | convolution fusion | flops 1616510976 | bytes 8388608 | tf_op jit(solution)/shard_map/dot_general | solution.py:123
  (312 shorter events, 130.8 us)
Async XLA Ops:
  6.5 86.9 %copy-start.6 = (f32[31,256]{1,0:T(8,128)S(1)}, f32[31,256]{1,0:T(8,128)}, u32[]{:S(2)}) copy-start(f32[31,256]{1,0:T(8,128)} %param.37) | copy-start | bytes 95236
  6.5 88.2 %copy-start.41 = (f32[256]{0:T(256)S(1)}, f32[256]{0:T(256)}, u32[]{:S(2)}) copy-start(f32[256]{0:T(256)} %param.33) | copy-start | bytes 3076
  6.5 45.0 %all-gather.31.cloned.1.call-start = ((), (), s32[]{:S(2)}) async-start(), calls=%async_computation.10 | async-start | bytes 1179648 | tf_op jit(solution)/shard_map/all_gather | solution.py:182
  7.3 84.8 %all-gather.35.cloned.1.call-start = ((), (), s32[]{:S(2)}) async-start(), calls=%async_computation.12 | async-start | bytes 1179648 | tf_op jit(solution)/shard_map/all_gather | solution.py:183
  8.0 113.1 %all-gather.15.cloned.1.call-start = ((), (), s32[]{:S(2)}) async-start(), calls=%async_computation.2 | async-start | bytes 3932160 | tf_op jit(solution)/shard_map/all_gather | solution.py:100
  8.7 154.7 %all-gather.19.cloned.1.call-start = ((), (), s32[]{:S(2)}) async-start(), calls=%async_computation.4 | async-start | bytes 1179648 | tf_op jit(solution)/shard_map/all_gather | solution.py:114
  9.3 195.1 %all-gather.23.cloned.1.call-start = ((), (), s32[]{:S(2)}) async-start(), calls=%async_computation.6 | async-start | bytes 1179648 | tf_op jit(solution)/shard_map/all_gather | solution.py:113
  9.9 235.5 %all-gather.21.cloned.1.call-start = ((), (), s32[]{:S(2)}) async-start(), calls=%async_computation.5 | async-start | bytes 1179648 | tf_op jit(solution)/shard_map/all_gather | solution.py:115
  10.5 113.4 %copy-start.7 = (f32[2048]{0:T(1024)S(1)}, f32[2048]{0:T(1024)}, u32[]{:S(2)}) copy-start(f32[2048]{0:T(1024)} %param.24) | copy-start | bytes 24580
  10.5 416.7 %all-gather.27.cloned.1.call-start = ((), (), s32[]{:S(2)}) async-start(), calls=%async_computation.8 | async-start | bytes 1179648 | tf_op jit(solution)/shard_map/all_gather | solution.py:117
  11.2 420.2 %all-gather.29.cloned.1.call-start = ((), (), s32[]{:S(2)}) async-start(), calls=%async_computation.9 | async-start | bytes 1179648 | tf_op jit(solution)/shard_map/all_gather | solution.py:118
  12.0 424.3 %all-gather.25.cloned.1.call-start = ((), (), s32[]{:S(2)}) async-start(), calls=%async_computation.7 | async-start | bytes 1179648 | tf_op jit(solution)/shard_map/all_gather | solution.py:116
  12.7 451.1 %all-gather.33.cloned.1.call-start = ((), (), s32[]{:S(2)}) async-start(), calls=%async_computation.11 | async-start | bytes 5242880 | tf_op jit(solution)/shard_map/all_gather | solution.py:187
  51.6 415.5 %all-gather.37.cloned.1.call-start = ((), (), s32[]{:S(2)}) async-start(), calls=%async_computation.13 | async-start | bytes 5242880 | tf_op jit(solution)/shard_map/all_gather | solution.py:188
  92.0 398.7 %all-gather.39.cloned.1.call-start = ((), (), s32[]{:S(2)}) async-start(), calls=%async_computation.14 | async-start | bytes 2359296 | tf_op jit(solution)/shard_map/all_gather | solution.py:120
  92.6 447.8 %all-gather.17.cloned.1.call-start = ((), (), s32[]{:S(2)}) async-start(), calls=%async_computation.3 | async-start | bytes 2359296 | tf_op jit(solution)/shard_map/all_gather | solution.py:119
  124.0 39.5 %copy-start.43 = (f32[768,256]{1,0:T(8,128)S(1)}, f32[768,256]{1,0:T(8,128)}, u32[]{:S(2)}) copy-start(f32[768,256]{1,0:T(8,128)} %param.34) | copy-start | bytes 2359300
  403.3 21.5 %copy-start.5 = (f32[2,128,128]{2,1,0:T(8,128)S(1)}, f32[2,128,128]{2,1,0:T(8,128)}, u32[]{:S(2)}) copy-start(f32[2,128,128]{2,1,0:T(8,128)} %param.35) | copy-start | bytes 393220
  403.4 22.4 %copy-start.42 = (f32[256]{0:T(256)S(1)}, f32[256]{0:T(256)}, u32[]{:S(2)}) copy-start(f32[256]{0:T(256)} %param.36) | copy-start | bytes 3076
  427.2 4.2 copy-start.3
  434.5 5.3 collective-permute-start
  436.3 3.6 copy-start.8
  436.3 3.6 copy-start.9
  436.3 3.6 copy-start.10
  436.3 3.6 copy-start.11
  436.3 3.6 copy-start.12
  436.3 3.6 copy-start.13
  436.4 3.6 copy-start.14
  440.2 9.0 %copy-start.39 = (f32[256]{0:T(256)S(1)}, f32[256]{0:T(256)}, u32[]{:S(2)}) copy-start(f32[256]{0:T(256)} %param.39) | copy-start | bytes 3076
  440.2 9.0 %copy-start.40 = (f32[256]{0:T(256)S(1)}, f32[256]{0:T(256)}, u32[]{:S(2)}) copy-start(f32[256]{0:T(256)} %param.38) | copy-start | bytes 3076
  440.2 9.3 %copy-start.4 = (bf16[768,256]{1,0:T(8,128)(2,1)S(1)}, bf16[768,256]{1,0:T(8,128)(2,1)}, u32[]{:S(2)}) copy-start(bf16[768,256]{1,0:T(8,128)(2,1)} %multiply_convert_fusion.1) | copy-start | bytes 1179652
  474.5 29.2 %all-to-all-start.1 = ((bf16[192,2,2048]{0,1,2:T(2,128)(2,1)}), bf16[192,2,2048]{0,1,2:T(2,128)(2,1)S(1)}, u32[]{:S(2)}, u32[]{:S(2)}) async-start(bf16[192,2,2048]{0,1,2:T(2,128)(2,1)} %copy.86), calls=%async_computation.1 | async-start | bytes 4194304 | tf_op jit(solution)/shard_map/all_to_all | solution.py:201
  (27 other events, 92.7 us)
Sparse Core Ops, SparseCore 0:
  9.4 42.1 all-gather.30
  53.6 38.3 all-gather.34
  93.6 27.5 all-gather.14
  123.1 40.2 all-gather.18
  165.4 38.9 all-gather.22
  206.4 38.9 all-gather.20
  247.6 38.9 all-gather.26
  288.7 38.9 all-gather.28
  329.9 38.9 all-gather.24
  370.3 33.1 all-gather.32
  405.1 34.4 all-gather.36
  441.6 49.0 all-gather.38
  492.8 47.5 all-gather.16
where the time goes:
time: 556 us; the launch traced here: 553 us
  waiting for transfers between devices  277 us (50%)
  matrix products  77.9 us (14%)
  blocking collectives  69.7 us (13%)
  other arithmetic  66.1 us (12%)
  local copies, waits for them, and re-layouts  41.3 us (7%)
  between operations  14.2 us (3%)
  starting transfers between devices  6.07 us (1%)
    all_gather x2, blocking collectives, prefix(): lax.all_gather(part.astype(kind), axis)  50 us
    dot_general x12, other arithmetic, block_step(): jnp.einsum('htd,hsd,htsd->hts', query, input_gate, weight, precision=high...  42.5 us
    all_gather x1, waiting for transfers between devices, local(): lax.all_gather(w_out_conv, 'sp', axis=1, tiled=True)  40.4 us
    all_gather x1, waiting for transfers between devices, local(): lax.all_gather(w_out_rec, 'sp', axis=1, tiled=True)  38.8 us
    all_gather x1, waiting for transfers between devices, local(): lax.all_gather(weights[1], 'sp', axis=0, tiled=True)  37 us
    all_gather x1, waiting for transfers between devices, local(): lax.all_gather(weights[0], 'sp', axis=0, tiled=True)  36.7 us
    all_gather x1, waiting for transfers between devices, local(): lax.all_gather(weights[2], 'sp', axis=0, tiled=True)  36.6 us
    all_gather x1, waiting for transfers between devices, local(): lax.all_gather(weights[6], 'sp', axis=0, tiled=True)  33 us
  transfers between devices with their start and end apart: 15, of which 9 were waited for; matrix products, arithmetic and copies ran while one was open for 32% of the time, Pallas kernels for 0%

commit v1 on v0

v1 whole, which is shorter than its diff:
```python
import functools

import jax
import jax.numpy as jnp
from jax import lax
from jax.experimental import pallas as pl
from jax.experimental.pallas import tpu as pltpu
from jax.sharding import PartitionSpec as P


HEAD = 128
KW = 31
RIM = 32
CHUNK = 128
EXTRA = 16
EPSILON = 1e-06

AXES = ("sp", "tp")
f32, bf16 = jnp.float32, jnp.bfloat16
HBM = pl.BlockSpec(memory_space=pltpu.HBM)
VMEM = pl.BlockSpec(memory_space=pltpu.VMEM)
SMEM = pl.BlockSpec(memory_space=pltpu.SMEM)
NT = (((1,), (1,)), ((), ()))
TN = (((0,), (0,)), ((), ()))


def normalize_rows(values, gain_vector):
    widened = values.astype(f32)
    scale = lax.rsqrt(jnp.mean(widened * widened, axis=-1, keepdims=True) + EPSILON)
    return (widened * scale * gain_vector).astype(bf16)


class Copy:
    def __init__(self, source, row, rows, to_row, to_lane=None, flag=None):
        self.source, self.row, self.rows = source, row, rows
        self.to_row, self.to_lane, self.flag = to_row, to_lane, flag

    def run(self, act, place, sources, target, semaphore):
        source = sources[self.source]
        rows = self.to_row if isinstance(self.to_row, int) else self.to_row(*place)
        if not isinstance(rows, int):
            rows = pl.multiple_of(rows, 16)
        if self.to_lane is None:
            there = target.at[pl.ds(rows, self.rows), :]
        else:
            lane = pl.multiple_of(self.to_lane(*place), HEAD)
            there = target.at[pl.ds(rows, self.rows), pl.ds(lane, source.shape[1])]

        def go():
            here = source.at[pl.ds(self.row, self.rows), :]
            getattr(pltpu.make_async_copy(here, there, semaphore), act)()

        if self.flag is None:
            go()
        else:
            pl.when(self.flag(*place))(go)


def run_all(act, copies, place, sources, target, semaphores, first=0):
    for k, copy in enumerate(copies):
        copy.run(act, place, sources, target, semaphores.at[first + k])


def where_am_i(scalars):
    return scalars[0], scalars[1], scalars[2]


def params():
    return pltpu.CompilerParams(vmem_limit_bytes=56 * 1024 * 1024)


def cost(flops, moved):
    return pl.CostEstimate(flops=int(flops), bytes_accessed=int(moved), transcendentals=0)


def project(rows, depth, token_groups, n_tokens, weight_copies, n_weights):
    size = rows // len(token_groups)

    def body(scalars, *refs):
        tokens, refs = refs[:n_tokens], refs[n_tokens:]
        weights, refs = refs[:n_weights], refs[n_weights:]
        gated, ordered, token_v, weight_v, semaphores, out_semaphores = refs
        place = where_am_i(scalars)
        run_all("start", weight_copies, place, weights, weight_v, semaphores)
        first = len(weight_copies)
        for _, copies in token_groups:
            run_all("start", copies, place, tokens, token_v, semaphores, first)
            first += len(copies)
        run_all("wait", weight_copies, place, weights, weight_v, semaphores)
        first = len(weight_copies)
        writes = []
        for k, (start, copies) in enumerate(token_groups):
            run_all("wait", copies, place, tokens, token_v, semaphores, first)
            first += len(copies)
            block = pl.ds(pl.multiple_of(start(*place), 16), size)
            write = pltpu.make_async_copy(
                token_v.at[block, :], ordered.at[block, :], out_semaphores.at[k]
            )
            write.start()
            writes.append(write)
            raw = jnp.dot(token_v[block, :], weight_v[...], preferred_element_type=f32)
            raw = raw.astype(bf16).astype(f32)
            gated[block, :] = (raw[:, :HEAD] * jax.nn.sigmoid(raw[:, HEAD:])).astype(bf16)
        for write in writes:
            write.wait()

    n_copies = len(weight_copies) + sum(len(copies) for _, copies in token_groups)
    return pl.pallas_call(
        body,
        out_shape=(
            jax.ShapeDtypeStruct((rows, HEAD), bf16),
            jax.ShapeDtypeStruct((rows, depth), bf16),
        ),
        in_specs=[SMEM] + [HBM] * (n_tokens + n_weights),
        out_specs=(VMEM, HBM),
        scratch_shapes=[
            pltpu.VMEM((rows, depth), bf16),
            pltpu.VMEM((depth, 2 * HEAD), bf16),
            pltpu.SemaphoreType.DMA((n_copies,)),
            pltpu.SemaphoreType.DMA((len(token_groups),)),
        ],
        compiler_params=params(),
        cost_estimate=cost(2 * rows * depth * 2 * HEAD, rows * depth * 4),
        name="project",
    )


def recurrence(rows, half, n_decays):
    def body(scalars, raw, rate, *refs):
        decays, (local_out, running_query, packed) = refs[:n_decays], refs[n_decays:]
        at_or_before = lax.broadcasted_iota(
            jnp.int32, (CHUNK, CHUNK), 0
        ) >= lax.broadcasted_iota(jnp.int32, (CHUNK, CHUNK), 1)
        lower = at_or_before.astype(bf16)

        def step(side, k, carry):
            state, before = carry
            within = pl.ds(pl.multiple_of(k * CHUNK, CHUNK), CHUNK)
            block = pl.ds(pl.multiple_of(side * half + k * CHUNK, CHUNK), CHUNK)
            shift = decays[0][within, :]
            if n_decays > 1:
                shift = jnp.where(scalars[1] == side, shift, decays[1][within, :].astype(f32))
            forget = raw[block, :HEAD].astype(f32)
            values = raw[block, HEAD : 2 * HEAD]
            query = raw[block, 2 * HEAD :].astype(f32)
            query = query * jax.nn.sigmoid(query)
            gate = rate[...] * jax.nn.sigmoid(-forget)
            log_decay = jnp.log1p(-gate) + shift
            high = log_decay.astype(bf16)
            rest = log_decay - high.astype(f32)
            middle = rest.astype(bf16)
            low = (rest - middle.astype(f32)).astype(bf16)
            summed = jnp.dot(
                lower, jnp.concatenate([high, middle, low], axis=1), preferred_element_type=f32
            )
            cumulative = summed[:, :HEAD] + (summed[:, HEAD : 2 * HEAD] + summed[:, 2 * HEAD :])
            centre = cumulative[CHUNK // 2 - 1 : CHUNK // 2, :]
            final = cumulative[CHUNK - 1 :, :]
            query_scaled = query * jnp.exp(cumulative - centre)
            gate_scaled = gate * jnp.exp(centre - cumulative)
            scores = lax.dot_general(
                query_scaled.astype(bf16),
                gate_scaled.astype(bf16),
                NT,
                preferred_element_type=f32,
            )
            scores = jnp.where(at_or_before, scores, 0.0).astype(bf16)
            from_state = (query_scaled * jnp.exp(centre)).astype(bf16)
            local_out[block, :] = jnp.dot(
                scores, values, preferred_element_type=f32
            ) + lax.dot_general(from_state, state.astype(bf16), NT, preferred_element_type=f32)
            running_query[block, :] = (query_scaled * jnp.exp(centre + before)).astype(bf16)
            kept = (gate_scaled * jnp.exp(final - centre)).astype(bf16)
            added = lax.dot_general(values, kept, TN, preferred_element_type=f32)
            return state * jnp.exp(final) + added, before + final

        carry = (jnp.zeros((HEAD, HEAD), f32), jnp.zeros((1, HEAD), f32))
        for side in range(n_decays):
            carry = lax.fori_loop(
                0, half // CHUNK, functools.partial(step, side), carry, unroll=3
            )
        state, total = carry
        decay = jnp.exp(total)
        high = decay.astype(bf16).astype(f32)
        packed[:HEAD, :] = state.astype(bf16)
        row = lax.broadcasted_iota(jnp.int32, (EXTRA, HEAD), 0)
        packed[HEAD:, :] = jnp.where(
            row == 0, high, jnp.where(row == 1, decay - high, 0.0)
        ).astype(bf16)

    return pl.pallas_call(
        body,
        out_shape=(
            jax.ShapeDtypeStruct((rows, HEAD), f32),
            jax.ShapeDtypeStruct((rows, HEAD), bf16),
            jax.ShapeDtypeStruct((HEAD + EXTRA, HEAD), bf16),
        ),
        in_specs=[SMEM] + [VMEM] * (2 + n_decays),
        out_specs=(VMEM, VMEM, VMEM),
        compiler_params=params(),
        cost_estimate=cost(2 * rows * HEAD * HEAD * 50, rows * HEAD * 16),
        name="recurrence",
    )


def heads(rows, depth, weight_copies, n_weights):
    size = rows // 4

    def body(scalars, tokens, *refs):
        weights, (raw_out, outgate, weight_v, semaphores) = refs[:n_weights], refs[n_weights:]

        @pl.when(pl.program_id(0) == 0)
        def _():
            for act in ("start", "wait"):
                run_all(act, weight_copies, where_am_i(scalars), weights, weight_v, semaphores)

        raw = jnp.dot(tokens[...], weight_v[...], preferred_element_type=f32).astype(bf16)
        raw_out[...] = raw[:, : 3 * HEAD]
        outgate[...] = raw[:, 3 * HEAD :]

    return pl.pallas_call(
        body,
        grid=(rows // size,),
        out_shape=(
            jax.ShapeDtypeStruct((rows, 3 * HEAD), bf16),
            jax.ShapeDtypeStruct((rows, HEAD), bf16),
        ),
        in_specs=[SMEM, pl.BlockSpec((size, depth), lambda i: (i, 0))] + [HBM] * n_weights,
        out_specs=(
            pl.BlockSpec((size, 3 * HEAD), lambda i: (i, 0)),
            pl.BlockSpec((size, HEAD), lambda i: (i, 0)),
        ),
        scratch_shapes=[
            pltpu.VMEM((depth, 4 * HEAD), bf16),
            pltpu.SemaphoreType.DMA((len(weight_copies),)),
        ],
        compiler_params=params(),
        cost_estimate=cost(2 * rows * depth * 4 * HEAD, rows * depth * 2),
        name="heads",
    )


def convolution(rows):
    def body(gated, previous, taps, gain, bias, out, extended):
        extended[:RIM, :] = previous[...].astype(f32)
        extended[RIM:, :] = gated[...].astype(f32)

        def step(k, carry):
            base = pl.multiple_of(k * CHUNK, CHUNK)
            total = jnp.zeros((CHUNK, HEAD), f32)
            for tap in range(KW):
                window = extended[pl.ds(base + RIM - KW + 1 + tap, CHUNK), :]
                total = total + taps[tap : tap + 1, :] * window
            out[pl.ds(base, CHUNK), :] = total.astype(bf16)
            return carry

        lax.fori_loop(0, rows // CHUNK, step, 0)
        row = lax.broadcasted_iota(jnp.int32, (EXTRA, HEAD), 0)
        small = jnp.zeros((EXTRA, HEAD), f32)
        for k, part in enumerate(split_three(gain[...]) + split_three(bias[...])):
            small = jnp.where(row == k, part.astype(f32), small)
        out[rows:, :] = small.astype(bf16)

    return pl.pallas_call(
        body,
        out_shape=jax.ShapeDtypeStruct((rows + EXTRA, HEAD), bf16),
        in_specs=[VMEM] * 5,
        out_specs=VMEM,
        scratch_shapes=[pltpu.VMEM((rows + RIM, HEAD), f32)],
        compiler_params=params(),
        cost_estimate=cost(2 * rows * HEAD * KW * 200, rows * HEAD * 8),
    )


def finish(rows, n_states):
    def body(scalars, local_out, running_query, outgate, initial, head_gain, *refs):
        states, out = refs[:n_states], refs[n_states]
        state = initial[...].T
        for k in reversed(range(n_states)):
            tail = states[k][HEAD:, :].astype(f32)
            decay = tail[0:1, :] + tail[1:2, :]
            state = jnp.where(
                scalars[0] > k, state * decay + states[k][:HEAD, :].astype(f32), state
            )
        state = state.astype(bf16)
        size = min(256, rows)
        for k in range(rows // size):
            block = pl.ds(k * size, size)
            head_out = local_out[block, :] + lax.dot_general(
                running_query[block, :], state, NT, preferred_element_type=f32
            )
            scale = lax.rsqrt(jnp.mean(head_out * head_out, axis=-1, keepdims=True) + EPSILON)
            gate = outgate[block, :].astype(f32)
            out[block, :] = (
                head_out * scale * head_gain[...] * (gate * jax.nn.sigmoid(gate))
            ).astype(bf16)

    return pl.pallas_call(
        body,
        out_shape=jax.ShapeDtypeStruct((rows, HEAD), bf16),
        in_specs=[SMEM] + [VMEM] * (5 + n_states),
        out_specs=VMEM,
        compiler_params=params(),
        cost_estimate=cost(2 * rows * HEAD * HEAD * 20, rows * HEAD * 12),
        name="finish",
    )


def activate(rows, channels, groups, tail_copies, n_pieces):
    size = rows // len(groups)

    def body(scalars, *refs):
        pieces, refs = refs[:n_pieces], refs[n_pieces:]
        out, wide_v, tail_v, semaphores, tail_semaphores = refs
        place = where_am_i(scalars)
        step = pl.program_id(0)

        @pl.when(step == 0)
        def _():
            run_all("start", tail_copies, place, pieces, tail_v, tail_semaphores)
            for k, copies in enumerate(groups):
                run_all("start", copies, place, pieces, wide_v, semaphores.at[k])
            run_all("wait", tail_copies, place, pieces, tail_v, tail_semaphores)

        for k, copies in enumerate(groups):

            @pl.when(step == k)
            def _():
                run_all("wait", copies, place, pieces, wide_v, semaphores.at[k])

        block = pl.ds(pl.multiple_of(step * size, size), size)
        squares = jnp.zeros((size, HEAD), f32)
        for u in range(channels // HEAD):
            value = wide_v[block, u * HEAD : (u + 1) * HEAD].astype(f32)
            squares = squares + value * value
        scale = lax.rsqrt(jnp.sum(squares, axis=-1, keepdims=True) / channels + EPSILON)
        for u in range(channels // HEAD):
            lanes = slice(u * HEAD, (u + 1) * HEAD)
            small = tail_v[:, lanes].astype(f32)
            gain = small[0:1, :] + small[1:2, :] + small[2:3, :]
            bias = small[3:4, :] + small[4:5, :] + small[5:6, :]
            value = wide_v[block, lanes].astype(f32) * scale * gain + bias
            out[:, lanes] = (value * jax.nn.sigmoid(value)).astype(bf16)

    return pl.pallas_call(
        body,
        grid=(len(groups),),
        out_shape=jax.ShapeDtypeStruct((rows, channels), bf16),
        in_specs=[SMEM] + [HBM] * n_pieces,
        out_specs=pl.BlockSpec((size, channels), lambda i: (i, 0)),
        scratch_shapes=[
            pltpu.VMEM((rows, channels), bf16),
            pltpu.VMEM((EXTRA, channels), bf16),
            pltpu.SemaphoreType.DMA((len(groups), max(len(copies) for copies in groups))),
            pltpu.SemaphoreType.DMA((len(tail_copies),)),
        ],
        compiler_params=params(),
        cost_estimate=cost(rows * channels * 2000, rows * channels * 4),
        name="activate",
    )


def combine(rows, start, lane, depth, channels, width, wide, copies, counts):
    gate_copies, out_copies, rec_copies = copies
    n_weights, n_outs, n_rec = counts
    blocks = 3 if rows % (3 * 128) == 0 else 2
    size = rows // blocks

    def body(scalars, tokens, conv, *refs):
        weights, refs = refs[:n_weights], refs[n_weights:]
        outs, refs = refs[:n_outs], refs[n_outs:]
        rec, refs = refs[:n_rec], refs[n_rec:]
        out, gate_v, out_v, rec_v, token_v, conv_v, semaphores = refs
        place = where_am_i(scalars)
        base = start(*place)
        column = pl.multiple_of(lane(*place) * width, HEAD)
        n_gate, n_out = len(gate_copies), len(out_copies)
        last = n_gate + n_out + len(rec_copies)

        def from_row(source, target, row, count, semaphore):
            rows_there = pl.ds(pl.multiple_of(base + row, 16), count)
            return pltpu.make_async_copy(
                source.at[rows_there, :], target.at[pl.ds(row, count), :], semaphores.at[semaphore]
            )

        conv_copy = from_row(conv, conv_v, 0, rows, last)
        token_copies = [
            from_row(tokens, token_v, k * size, size, last + 1 + k) for k in range(blocks)
        ]
        run_all("start", out_copies, place, outs, out_v, semaphores, n_gate)
        conv_copy.start()
        run_all("start", rec_copies, place, rec, rec_v, semaphores, n_gate + n_out)
        run_all("start", gate_copies, place, weights, gate_v, semaphores)
        for copy in token_copies:
            copy.start()
        run_all("wait", out_copies, place, outs, out_v, semaphores, n_gate)
        conv_copy.wait()
        y_conv = jnp.dot(conv_v[...], out_v[:, width:], preferred_element_type=f32).astype(bf16)
        run_all("wait", rec_copies, place, rec, rec_v, semaphores, n_gate + n_out)
        y_rec = jnp.dot(rec_v[...], out_v[:, :width], preferred_element_type=f32).astype(bf16)
        run_all("wait", gate_copies, place, weights, gate_v, semaphores)
        for k, copy in enumerate(token_copies):
            copy.wait()
            block = slice(k * size, (k + 1) * size)
            raw = jnp.dot(token_v[block, :], gate_v[...], preferred_element_type=f32)
            raw = raw.astype(bf16).astype(f32)
            merged = jax.nn.sigmoid(raw[:, :width]) * y_rec[block, :].astype(f32)
            merged = merged + jax.nn.sigmoid(raw[:, width:]) * y_conv[block, :].astype(f32)
            if wide == width:
                out[block, :] = merged.astype(bf16)
            else:
                out[block, pl.ds(column, width)] = merged.astype(bf16)

    n_copies = sum(len(group) for group in copies) + 1 + blocks
    return pl.pallas_call(
        body,
        out_shape=jax.ShapeDtypeStruct((rows, wide), bf16),
        in_specs=[SMEM] + [HBM] * (2 + n_weights + n_outs + n_rec),
        out_specs=VMEM,
        scratch_shapes=[
            pltpu.VMEM((depth, 2 * width), bf16),
            pltpu.VMEM((channels, 2 * width), bf16),
            pltpu.VMEM((rows, channels), bf16),
            pltpu.VMEM((rows, depth), bf16),
            pltpu.VMEM((rows, channels), bf16),
            pltpu.SemaphoreType.DMA((n_copies,)),
        ],
        compiler_params=params(),
        cost_estimate=cost(2 * rows * depth * 3 * width, rows * depth * 4),
        name="combine",
    )


def beside(rows, width):
    def body(scalars, theirs, mine, out):
        out[...] = theirs[...]

    return pl.pallas_call(
        body,
        out_shape=jax.ShapeDtypeStruct((rows, 2 * width), bf16),
        grid_spec=pltpu.PrefetchScalarGridSpec(
            num_scalar_prefetch=1,
            grid=(2,),
            in_specs=[pl.BlockSpec((rows // 2, width), lambda i, scalars: (i, 0)), HBM],
            out_specs=pl.BlockSpec((rows // 2, width), lambda i, scalars: (i, 1 - scalars[1])),
        ),
        input_output_aliases={2: 0},
        compiler_params=params(),
        name="beside",
    )


def split_three(vector):
    high = vector.astype(bf16)
    rest = vector - high.astype(f32)
    middle = rest.astype(bf16)
    return [high, middle, (rest - middle.astype(f32)).astype(bf16)]


def local(
    n_sp,
    n_tp,
    tokens,
    norm_gain,
    w_query,
    w_forget,
    w_input,
    w_outgate,
    w_conv_value,
    w_conv_gate,
    w_gate_rec,
    w_gate_conv,
    lower_bound,
    decay_shift,
    state_init,
    head_gain,
    conv_kernel,
    channel_gain,
    channel_bias,
    w_out_rec,
    w_out_conv,
):
    q = w_query.shape[1] // HEAD
    nz = n_sp // q
    depth = tokens.shape[1]
    channels = w_query.shape[1] * n_tp
    shard = tokens.shape[0]
    rows = shard * n_tp * q
    half = rows // q
    width = w_gate_rec.shape[1] // q
    direct = q == 2 and n_tp == 4 and nz == 4
    assert direct or q == 1
    s, t = lax.axis_index("sp"), lax.axis_index("tp")
    z, y = s // q, s % q
    own = y * n_tp + t

    def send(value, route):
        pairs = []
        for source in range(n_sp * n_tp):
            si, ti = source // n_tp, source % n_tp
            to = route(si // q, si % q, ti)
            if to is not None:
                pairs.append((source, (to[0] * q + to[1]) * n_tp + to[2]))
        return lax.ppermute(value, AXES, pairs)

    def up(k):
        return lambda a, b, c: (a + k, b, c) if a + k < nz else None

    def middle(a, b, c):
        return (3 - a, b, c) if a in (1, 2) else None

    def outwards(a, b, c):
        return ({1: 0, 2: 3}[a], b, c) if a in (1, 2) else None

    def other_y(a, b, c):
        return (a, 1 - b, c)

    def other_x(a, b, c):
        return (a, b, c ^ 2)

    def other_core(a, b, c):
        return (a, b, c ^ 1)

    def columns(ws, which):
        return jnp.concatenate(
            [
                lax.dynamic_slice_in_dim(w, which * (w.shape[1] // q), w.shape[1] // q, 1)
                for w in ws
            ],
            axis=1,
        )

    def own_columns(ws):
        if q == 1:
            return jnp.concatenate(ws, axis=1)
        theirs = send(columns(ws, 1 - y), other_y)
        mine = columns(ws, y)
        return jnp.concatenate([mine, theirs], axis=0)

    def along_z(piece, short=False):
        if not direct:
            return [lax.all_gather(piece, "sp", axis=0, tiled=True)]
        if short:
            return [piece] + [send(piece, lambda a, b, c: (a ^ k, b, c)) for k in range(1, nz)]
        outer = send(piece, lambda a, b, c: (a ^ 1, b, c))
        inner = send(piece, middle)
        outer_2 = send(inner, outwards)
        inner_2 = send(outer, middle)
        outer_3 = send(inner_2, outwards)
        return [piece, outer, inner, outer_2, inner_2, outer_3]

    def rows_of(scale, blocks, short=False):
        if not direct:
            return [Copy(0, 0, scale * nz, 0)]

        def copy(source, block, flag, row, count, within):
            return Copy(
                source,
                row,
                count,
                lambda z, y, own: block(z) * scale + within(y),
                flag=None if flag is None else lambda z, y, own: flag(z),
            )

        def inside(z):
            return (z == 1) | (z == 2)

        def at_an_end(z):
            return (z == 0) | (z == 3)

        near, far = (lambda z: jnp.where(z < 2, 2, 1)), (lambda z: jnp.where(z < 2, 3, 0))
        sources = (
            (0, lambda z: z, None),
            (1, lambda z: z ^ 1, None),
            (2, near, inside),
            (3, near, at_an_end),
            (4, far, inside),
            (5, far, at_an_end),
        )
        if short:
            sources = [(k, lambda z, k=k: z ^ k, None) for k in range(nz)]
        return [copy(*source, *block) for source in sources for block in blocks]

    def plane_gather(value, halves=False):
        size = value.shape[0]
        if not direct:
            everything = lax.all_gather(value, "tp", axis=0, tiled=False)
            return [everything[k] for k in range(n_tp)], [(k, 0, size, 0, k) for k in range(n_tp)]
        by_y, by_x = send(value, other_y), send(value, other_x)
        if halves:
            cut = size // 2
            top = send(by_x[:cut], other_y)
            bottom = send(by_y[cut:], other_x)
            arrays, parts = [], []
            for array, row, place in (
                (value, 0, 0),
                (by_x, 0, 2),
                (by_y, 0, n_tp),
                (top, 0, n_tp + 2),
                (bottom, cut, n_tp + 2),
            ):
                for piece, core in ((array, 0), (send(array, other_core), 1)):
                    parts.append((len(arrays), 0, piece.shape[0], row, place ^ core))
                    arrays.append(piece)
            return arrays, parts
        across = send(value, lambda a, b, c: (a, 1 - b, c ^ 2))
        near = send(value, other_core)
        others = jnp.concatenate([by_x, by_y, across], axis=0)
        others = send(others, other_core)
        arrays = [value, by_x, by_y, across, near, others]
        places = (0, 2, n_tp, n_tp + 2, 1)
        parts = [(k, 0, size, 0, place) for k, place in enumerate(places)]
        parts += [(5, k * size, size, 0, place ^ 1) for k, place in enumerate(places[1:4])]
        return arrays, parts

    def absolute(place, own):
        return place ^ own if direct else place

    def token_copy(array, row, count, within, place):
        return Copy(
            array, row, count, lambda z, y, own: absolute(place, own) * shard + within
        )

    normed = normalize_rows(tokens, norm_gain)
    piece_a = own_columns((w_conv_value, w_conv_gate))
    token_arrays, token_parts = plane_gather(normed, True)
    weights_a = along_z(piece_a)
    if q == 1:
        decays = [decay_shift]
    else:
        theirs = columns((decay_shift,), 1 - y).astype(bf16)
        decays = [columns((decay_shift,), y), send(theirs, other_y)]

    def unit(vector):
        return lax.dynamic_slice_in_dim(vector, y * HEAD, HEAD, vector.ndim - 1)

    here = jnp.stack([z, y, own]).astype(jnp.int32)
    sub = depth // n_sp
    inner = [(k * sub, sub, lambda y, k=k: (y ^ k) * sub) for k in range(q)]
    token_groups = [
        (
            lambda z, y, own, k=k: (y ^ k) * half,
            [token_copy(*part) for part in token_parts if part[-1] // n_tp == k],
        )
        for k in range(q)
    ]
    gated, ordered = project(
        rows,
        depth,
        token_groups,
        len(token_arrays),
        rows_of(sub * q, inner),
        len(weights_a),
    )(here, *token_arrays, *weights_a)
    previous = send(gated[rows - RIM :], up(1))
    taps = jnp.concatenate([unit(conv_kernel), jnp.zeros((RIM - KW, HEAD), f32)])
    conv_out = convolution(rows)(
        gated, previous, taps, unit(channel_gain)[None, :], unit(channel_bias)[None, :]
    )
    conv_arrays, conv_parts = plane_gather(conv_out)

    piece_b = own_columns((w_forget, w_input, w_query, w_outgate))
    weights_b = along_z(piece_b)
    raw, outgate = heads(rows, depth, rows_of(sub * q, inner), len(weights_b))(
        here, ordered, *weights_b
    )
    local_out, running_query, packed = recurrence(rows, half, q)(
        here, raw, 1.0 - unit(lower_bound)[None, :], *decays
    )
    if direct:
        states = [send(packed, up(k)) for k in range(1, nz)]
    else:
        gathered = lax.all_gather(packed, "sp", axis=0, tiled=False)
        states = [
            lax.dynamic_index_in_dim(gathered, jnp.maximum(z - k, 0), 0, False)
            for k in range(1, nz)
        ]
    mixed_rec = finish(rows, nz - 1)(
        here,
        local_out,
        running_query,
        outgate,
        lax.dynamic_index_in_dim(state_init, y, 0, False),
        unit(head_gain)[None, :],
        *states,
    )
    rec_arrays, rec_parts = plane_gather(mixed_rec)

    gates = own_columns((w_gate_rec, w_gate_conv))
    outs = jnp.concatenate([w_out_rec, w_out_conv], axis=1)
    if direct:
        outs = send(outs, lambda a, b, c: (c, b, a))
        weights_c, weights_d = along_z(gates), along_z(outs, True)
    else:
        weights_c = along_z(gates)
        whole = [
            lax.all_gather(lax.all_gather(w, "sp", axis=1, tiled=True), "tp", axis=0, tiled=True)
            for w in (w_out_rec, w_out_conv)
        ]
        whole = [lax.dynamic_slice_in_dim(w, t * width, width, 1) for w in whole]
        weights_d = [jnp.concatenate(whole, axis=1)]

    def lane_of(place):
        def lane(z, y, own):
            block = absolute(place, own)
            return ((block % n_tp) * q + block // n_tp) * HEAD

        return lane

    n_groups = max(1, rows // 256)
    size = rows // n_groups
    groups, tail_copies = [[] for _ in range(n_groups)], []
    for array, row, count, within, place in conv_parts:
        for k in range(n_groups):
            if within <= k * size < within + count:
                groups[k].append(Copy(array, row + k * size, size, k * size, lane_of(place)))
        if within + count > rows:
            tail_copies.append(Copy(array, row + rows, EXTRA, 0, lane_of(place)))
    mixed_conv = activate(rows, channels, groups, tail_copies, len(conv_arrays))(
        here, *conv_arrays
    )

    gate_copies = rows_of(sub * q, inner)
    out_rows = channels // nz
    out_copies = rows_of(out_rows, [(0, out_rows, lambda y: 0)], True)

    def final_rows(keep):
        rec_copies = []
        for array, row, count, within, place in rec_parts:
            for side in range(q):
                if within <= side * half < within + count:
                    flag = None if q == 1 else lambda z, y, own, side=side: (y ^ keep) == side
                    rec_copies.append(
                        Copy(array, row + side * half, half, 0, lane_of(place), flag)
                    )
        return combine(
            half,
            lambda z, y, own: (y ^ keep) * half,
            lambda z, y, own: y if q > 1 and keep == 0 else 0,
            depth,
            channels,
            width,
            width * q if keep == 0 else width,
            (gate_copies, out_copies, rec_copies),
            (len(weights_c), len(weights_d), len(rec_arrays)),
        )(here, ordered, mixed_conv, *weights_c, *weights_d, *rec_arrays)

    if q == 1:
        return final_rows(0)
    theirs = send(final_rows(1), other_y)
    return beside(half, width)(here, theirs, final_rows(0))


def solution(mesh):
    in_specs = (
        P(("sp", "tp"), None),
        P(),
        P("sp", "tp"),
        P("sp", "tp"),
        P("sp", "tp"),
        P("sp", "tp"),
        P("sp", "tp"),
        P("sp", "tp"),
        P("sp", "tp"),
        P("sp", "tp"),
        P("tp"),
        P("sp", "tp"),
        P("tp", None, None),
        P("tp"),
        P(None, "tp"),
        P("tp"),
        P("tp"),
        P("tp", "sp"),
        P("tp", "sp"),
    )
    step = functools.partial(local, mesh.shape["sp"], mesh.shape["tp"])
    step = jax.shard_map(
        step, mesh=mesh, in_specs=in_specs, out_specs=P("sp", "tp"), check_vma=False
    )
    return step
```

time: 556 us -> 232 us (0.42)
  waiting for transfers between devices: 277 us -> 75.2 us
  matrix products: 77.9 us -> 0 us
  starting transfers between devices: 6.07 us -> 78.7 us
  blocking collectives: 69.7 us -> 0 us
  other arithmetic: 66.1 us -> 5.03 us
  Pallas kernels: 0 us -> 54.4 us
  local copies, waits for them, and re-layouts: 41.3 us -> 17.4 us
  between operations: 14.2 us -> 0.71 us
    all_gather x13 -> x0, waiting for transfers between devices: 261 us -> none  [the longest x1 40.4 us: local(): lax.all_gather(w_out_conv, 'sp', axis=1, tiled=True)]
    dot_general x47 -> x0, matrix products: 77.9 us -> none  [the longest x8 31.1 us: local(): jnp.dot(normed, portion, preferred_element_type=jnp.float32)]
    ppermute x1 -> x47, starting transfers between devices: 1.79 us -> 78.7 us  [send(): return lax.ppermute(value, AXES, pairs)]
    ppermute x1 -> x47, waiting for transfers between devices: 0.01 us -> 75.2 us  [send(): return lax.ppermute(value, AXES, pairs)]
    pallas_call x0 -> x9, Pallas kernels: none -> 54.4 us  [the longest x2 15.5 us: final_rows(): combine(half, lambda z, y, own: (y ^ keep) * half, lambda z, y, own: y if...]
    all_gather x2 -> x0, blocking collectives: 50 us -> none  [prefix(): lax.all_gather(part.astype(kind), axis)]
    dot_general x12 -> x0, other arithmetic: 42.5 us -> none  [block_step(): jnp.einsum('htd,hsd,htsd->hts', query, input_gate, weight, precision=high...]
    squeeze x24 -> x1, local copies, waits for them, and re-layouts: 20.9 us -> 1.45 us  [local(): lax.dynamic_index_in_dim(state_init, y, 0, False)]
  transfers between devices with their start and end apart: 15 -> 47, of which waited for: 9 -> 15; matrix products, arithmetic and copies ran while one was open for 32% -> 7% of each run, Pallas kernels for 0% -> 19%
where the time goes in v1:
time: 232 us; the launch traced here: 231 us
  starting transfers between devices  78.7 us (34%)
  waiting for transfers between devices  75.2 us (32%)
  Pallas kernels  54.4 us (23%)
  local copies, waits for them, and re-layouts  17.4 us (7%)
  other arithmetic  5.03 us (2%)
    ppermute x47, starting transfers between devices, send(): return lax.ppermute(value, AXES, pairs)  78.7 us
    ppermute x47, waiting for transfers between devices, send(): return lax.ppermute(value, AXES, pairs)  75.2 us
    pallas_call x2, Pallas kernels, final_rows(): combine(half, lambda z, y, own: (y ^ keep) * half, lambda z, y, own: y if...  15.5 us
    pallas_call x1, Pallas kernels, local(): heads(rows, depth, rows_of(sub * q, inner), len(weights_b))  8.67 us
    pallas_call x1, Pallas kernels, local(): project(rows, depth, token_groups, len(token_arrays), rows_of(sub * q, in...  7.46 us
    pallas_call x1, Pallas kernels, local(): activate(rows, channels, groups, tail_copies, len(conv_arrays))  7.22 us
    pallas_call x1, Pallas kernels, local(): recurrence(rows, half, q)  6.86 us
    unnamed x88, local copies, waits for them, and re-layouts  5.9 us
  transfers between devices with their start and end apart: 47, of which 15 were waited for; matrix products, arithmetic and copies ran while one was open for 7% of the time, Pallas kernels for 19%

profile of v1, /device:TPU:0, one launch (start us, length us, event | category | flops | bytes accessed | tf_op | source)
XLA Modules:
  0.0 231.4 jit_solution(4911770644498865053)
XLA Ops:
  1.2 3.1 %collective-permute-start.9 = (bf16[256,256]{1,0:T(8,128)(2,1)S(1)}, bf16[256,256]{1,0:T(8,128)(2,1)S(1)}, u32[]{:S(2)}, u32[]{:S(2)}) collective-permute-start(bf16[256,256]{1,0:T(8,128)(2,1)S(1)} %pad_maximum_fusion.8), channel_id=1, source_target_pairs={{0,4},{1,5},{2,6},{3,7},{4,0},{5,1},{6,2},{7,3},{8,12},{9,13},{10,... | collective-permute-start | bytes 393224 | tf_op jit(solution)/shard_map/ppermute | solution.py:504
  7.8 1.9 collective-permute-start.10
  9.7 1.6 collective-permute-start.31
  13.1 2.2 collective-permute-done.10.refs_11_
  16.7 2.2 collective-permute-done.31
  19.8 3.7 %collective-permute-start.32 = (bf16[512,512]{1,0:T(8,128)(2,1)}, bf16[512,512]{1,0:T(8,128)(2,1)}, u32[]{:S(2)}, u32[]{:S(2)}) collective-permute-start(bf16[512,512]{1,0:T(8,128)(2,1)} %pad_maximum_fusion.3.refs_0_), channel_id=1, source_target_pairs={{0,8},{1,9},{2,10},{3,11},{4,12},{5,13},{6,14},{7,15},{8,0},{9,1},... | collective-permute-start | bytes 1572872 | tf_op jit(solution)/shard_map/ppermute | solution.py:504
  27.1 12.9 %collective-permute-done.12.refs_13_ = bf16[512,256]{1,0:T(8,128)(2,1)} collective-permute-done((bf16[512,256]{1,0:T(8,128)(2,1)}, bf16[512,256]{1,0:T(8,128)(2,1)}, u32[]{:S(2)}, u32[]{:S(2)}) %collective-permute-start.12) | collective-permute-done | bytes 262176 | tf_op jit(solution)/shard_map/ppermute | solution.py:504
  41.4 1.6 collective-permute-start.5
  43.0 1.8 constant_dynamic-slice_fusion.11
  52.3 2.3 collective-permute-done.7.refs_8_
  63.9 7.5 %project.1 = (bf16[1536,128]{1,0:T(8,128)(2,1)}, bf16[1536,2048]{1,0:T(8,128)(2,1)}) custom-call(s32[3]{0:T(128)} %pad_add_fusion.scalars, bf16[192,2048]{1,0:T(8,128)(2,1)} %copy-done.7, bf16[192,2048]{1,0:T(8,128)(2,1)} %collective-permute-done.refs_1_, bf16[192,2048]{1,0:T(8,128)(2,1)} %copy-done.13, bf16[192,2048]{1,0:T(8,128)(2,1)} %collective-permute-done.2.refs_3_, ...), custom_call_target="tpu_custom_call" | custom-call | flops 1610612736 | bytes 12582912 | tf_op jit(solution)/shard_map/project/pallas_call | solution.py:647
  72.1 12.0 %collective-permute-start.15 = (bf16[32,128]{1,0:T(8,128)(2,1)S(1)}, bf16[32,128]{1,0:T(8,128)(2,1)S(1)}, u32[]{:S(2)}, u32[]{:S(2)}) collective-permute-start(bf16[32,128]{1,0:T(8,128)(2,1)S(1)} %slice.11), channel_id=1, source_target_pairs={{0,8},{1,9},{2,10},{3,11},{4,12},{5,13},{6,14},{7,15},{8,16},{9,17... | collective-permute-start | bytes 24584 | tf_op jit(solution)/shard_map/ppermute | solution.py:504
  86.1 3.6 %shard_map.181.refs_0_ = bf16[1552,128]{1,0:T(8,128)(2,1)} custom-call(bf16[1536,128]{1,0:T(8,128)(2,1)} %get-tuple-element.13.gated, bf16[32,128]{1,0:T(8,128)(2,1)} %copy-done.41, f32[32,128]{1,0:T(8,128)} %concatenate.42.taps, f32[1,128]{1,0:T(1,128)} %get-tuple-element.42.gain, f32[1,128]{1,0:T(1,128)} %get-tuple-element.41.bias), custom_call_target="tpu_custom_call" | custom-call | flops 2437939200 | bytes 1572864 | tf_op jit(solution)/shard_map/pallas_call | solution.py:657
  89.7 9.8 %collective-permute-start.16 = (bf16[1552,128]{1,0:T(8,128)(2,1)}, bf16[1552,128]{1,0:T(8,128)(2,1)S(1)}, u32[]{:S(2)}, u32[]{:S(2)}) collective-permute-start(bf16[1552,128]{1,0:T(8,128)(2,1)} %shard_map.181.refs_0_), channel_id=1, source_target_pairs={{0,2},{1,3},{2,0},{3,1},{4,6},{5,7},{6,4},{7,5},{8,10},{9,11},{10,... | collective-permute-start | bytes 1191944 | tf_op jit(solution)/shard_map/ppermute | solution.py:504
  100.4 8.7 %heads.1 = (bf16[1536,384]{1,0:T(8,128)(2,1)}, bf16[1536,128]{1,0:T(8,128)(2,1)}) custom-call(s32[3]{0:T(128)} %pad_add_fusion.scalars, bf16[1536,2048]{1,0:T(8,128)(2,1)} %get-tuple-element.12.tokens, bf16[512,512]{1,0:T(8,128)(2,1)} %pad_maximum_fusion.3.refs_0_, bf16[512,512]{1,0:T(8,128)(2,1)} %collective-permute-done.32.refs_1_, ...), custom_call_target="tpu_custom_call" | custom-call | flops 3221225472 | bytes 6291456 | tf_op jit(solution)/shard_map/heads/pallas_call | solution.py:664
  109.8 6.9 %recurrence.1 = (f32[1536,128]{1,0:T(8,128)}, bf16[1536,128]{1,0:T(8,128)(2,1)}, bf16[144,128]{1,0:T(8,128)(2,1)}) custom-call(s32[3]{0:T(128)} %pad_add_fusion.scalars, bf16[1536,384]{1,0:T(8,128)(2,1)} %get-tuple-element.14.raw, f32[1,128]{1,0:T(1,128)} %subtract_bitcast_fusion.rate, f32[768,128]{1,0:T(8,128)} %constant_dynamic-slice_fusion.refs_0_, ...), custom_call_target="tpu_custom_call" | custom-call | flops 2516582400 | bytes 3145728 | tf_op jit(solution)/shard_map/recurrence/pallas_call | solution.py:667
  118.6 5.5 %collective-permute-start.39 = (bf16[144,128]{1,0:T(8,128)(2,1)}, bf16[144,128]{1,0:T(8,128)(2,1)S(1)}, u32[]{:S(2)}, u32[]{:S(2)}) collective-permute-start(bf16[144,128]{1,0:T(8,128)(2,1)} %get-tuple-element.18), channel_id=1, source_target_pairs={{0,16},{1,17},{2,18},{3,19},{4,20},{5,21},{6,22},{7,23},{8,24},{9,... | collective-permute-start | bytes 110600 | tf_op jit(solution)/shard_map/ppermute | solution.py:504
  124.1 3.0 %collective-permute-start.40 = (bf16[144,128]{1,0:T(8,128)(2,1)}, bf16[144,128]{1,0:T(8,128)(2,1)S(1)}, u32[]{:S(2)}, u32[]{:S(2)}) collective-permute-start(bf16[144,128]{1,0:T(8,128)(2,1)} %get-tuple-element.18), channel_id=1, source_target_pairs={{0,24},{1,25},{2,26},{3,27},{4,28},{5,29},{6,30},{7,31}} | collective-permute-start | bytes 110600 | tf_op jit(solution)/shard_map/ppermute | solution.py:504
  127.2 2.0 collective-permute-done.40.refs_2_
  129.8 2.8 %finish.1.refs_10_ = bf16[1536,128]{1,0:T(8,128)(2,1)} custom-call(s32[3]{0:T(128)} %pad_add_fusion.scalars, f32[1536,128]{1,0:T(8,128)} %get-tuple-element.15.local_out, bf16[1536,128]{1,0:T(8,128)(2,1)} %get-tuple-element.16.running_query, bf16[1536,128]{1,0:T(8,128)(2,1)} %get-tuple-element.17.outgate, f32[128,128]{1,0:T(8,128)} %dynamic-slice_bitcast_fusion.initial, ...), custom_call_target="tpu_custom_call" | custom-call | flops 1006632960 | bytes 2359296 | tf_op jit(solution)/shard_map/finish/pallas_call | solution.py:678
  134.0 2.1 collective-permute-start.43
  136.2 8.6 %collective-permute-done.41.refs_11_ = bf16[1536,128]{1,0:T(8,128)(2,1)S(1)} collective-permute-done((bf16[1536,128]{1,0:T(8,128)(2,1)}, bf16[1536,128]{1,0:T(8,128)(2,1)S(1)}, u32[]{:S(2)}, u32[]{:S(2)}) %collective-permute-start.41) | collective-permute-done | bytes 393248 | tf_op jit(solution)/shard_map/ppermute | solution.py:504
  144.8 5.1 %collective-permute-done.42.refs_12_ = bf16[1536,128]{1,0:T(8,128)(2,1)S(1)} collective-permute-done((bf16[1536,128]{1,0:T(8,128)(2,1)}, bf16[1536,128]{1,0:T(8,128)(2,1)S(1)}, u32[]{:S(2)}, u32[]{:S(2)}) %collective-permute-start.42) | collective-permute-done | bytes 393248 | tf_op jit(solution)/shard_map/ppermute | solution.py:504
  150.1 3.6 %collective-permute-start.29 = (bf16[256,512]{1,0:T(8,128)(2,1)S(1)}, bf16[256,512]{1,0:T(8,128)(2,1)S(1)}, u32[]{:S(2)}, u32[]{:S(2)}) collective-permute-start(bf16[256,512]{1,0:T(8,128)(2,1)S(1)} %collective-permute-done.27.refs_6_), channel_id=1, source_target_pairs={{0,16},{1,17},{2,18},{3,19},{4,20},{5,21},{6,22},{7,23},{8,24},{9,... | collective-permute-start | bytes 786440 | tf_op jit(solution)/shard_map/ppermute | solution.py:504
  155.1 11.3 %collective-permute-done.29.refs_8_ = bf16[256,512]{1,0:T(8,128)(2,1)S(1)} collective-permute-done((bf16[256,512]{1,0:T(8,128)(2,1)S(1)}, bf16[256,512]{1,0:T(8,128)(2,1)S(1)}, u32[]{:S(2)}, u32[]{:S(2)}) %collective-permute-start.29) | collective-permute-done | bytes 262176 | tf_op jit(solution)/shard_map/ppermute | solution.py:504
  171.1 3.2 %collective-permute-start.30 = (bf16[256,512]{1,0:T(8,128)(2,1)S(1)}, bf16[256,512]{1,0:T(8,128)(2,1)}, u32[]{:S(2)}, u32[]{:S(2)}) collective-permute-start(bf16[256,512]{1,0:T(8,128)(2,1)S(1)} %collective-permute-done.27.refs_6_), channel_id=1, source_target_pairs={{0,24},{1,25},{2,26},{3,27},{4,28},{5,29},{6,30},{7,31},{8,16},{9,... | collective-permute-start | bytes 786440 | tf_op jit(solution)/shard_map/ppermute | solution.py:504
  174.3 7.2 %activate.1.conv = bf16[1536,1024]{1,0:T(8,128)(2,1)} custom-call(s32[3]{0:T(128)} %pad_add_fusion.scalars, bf16[1552,128]{1,0:T(8,128)(2,1)} %shard_map.181.refs_0_, bf16[1552,128]{1,0:T(8,128)(2,1)} %copy-done.23, bf16[1552,128]{1,0:T(8,128)(2,1)} %copy-done.24, bf16[1552,128]{1,0:T(8,128)(2,1)} %copy-done.25, bf16[1552,128]{1,0:T(8,128)(2,1)} %copy-done.36, ...), custom_call_target="tpu_custom_call" | custom-call | flops 3145728000 | bytes 6291456 | tf_op jit(solution)/shard_map/activate/pallas_call | solution.py:719
  181.8 15.0 %collective-permute-done.24.refs_3_ = bf16[512,512]{1,0:T(8,128)(2,1)S(1)} collective-permute-done((bf16[512,512]{1,0:T(8,128)(2,1)S(1)}, bf16[512,512]{1,0:T(8,128)(2,1)S(1)}, u32[]{:S(2)}, u32[]{:S(2)}) %collective-permute-start.24) | collective-permute-done | bytes 524320 | tf_op jit(solution)/shard_map/ppermute | solution.py:504
  196.8 11.2 %collective-permute-done.26.refs_5_ = bf16[512,512]{1,0:T(8,128)(2,1)S(1)} collective-permute-done((bf16[512,512]{1,0:T(8,128)(2,1)S(1)}, bf16[512,512]{1,0:T(8,128)(2,1)S(1)}, u32[]{:S(2)}, u32[]{:S(2)}) %collective-permute-start.26) | collective-permute-done | bytes 524320 | tf_op jit(solution)/shard_map/ppermute | solution.py:504
  210.0 7.7 %combine.2 = bf16[768,256]{1,0:T(8,128)(2,1)} custom-call(s32[3]{0:T(128)} %pad_add_fusion.scalars, bf16[1536,2048]{1,0:T(8,128)(2,1)} %get-tuple-element.12.tokens, bf16[1536,1024]{1,0:T(8,128)(2,1)} %activate.1.conv, bf16[512,512]{1,0:T(8,128)(2,1)} %copy-done.2, bf16[512,512]{1,0:T(8,128)(2,1)} %copy-done.8, bf16[512,512]{1,0:T(8,128)(2,1)} %copy-done.9, ...), custom_call_target="tpu_custom_call" | custom-call | flops 2415919104 | bytes 6291456 | tf_op jit(solution)/shard_map/combine/pallas_call | solution.py:736
  218.9 7.8 %combine.3.mine = bf16[768,512]{1,0:T(8,128)(2,1)} custom-call(s32[3]{0:T(128)} %pad_add_fusion.scalars, bf16[1536,2048]{1,0:T(8,128)(2,1)} %get-tuple-element.12.tokens, bf16[1536,1024]{1,0:T(8,128)(2,1)} %activate.1.conv, bf16[512,512]{1,0:T(8,128)(2,1)} %copy-done.2, bf16[512,512]{1,0:T(8,128)(2,1)} %copy-done.8, bf16[512,512]{1,0:T(8,128)(2,1)} %copy-done.9, ...), custom_call_target="tpu_custom_call" | custom-call | flops 2415919104 | bytes 6291456 | tf_op jit(solution)/shard_map/combine/pallas_call | solution.py:736
  229.0 2.4 %beside.1 = bf16[768,512]{1,0:T(8,128)(2,1)} custom-call(s32[3]{0:T(128)} %pad_add_fusion.scalars, bf16[768,256]{1,0:T(8,128)(2,1)} %copy-done.26, bf16[768,512]{1,0:T(8,128)(2,1)} %combine.3.mine), custom_call_target="tpu_custom_call", output_to_operand_aliasing={{}: (2, {})} | custom-call | tf_op jit(solution)/shard_map/beside/pallas_call | solution.py:751
  (187 shorter events, 50.6 us)
Async XLA Ops:
  5.9 19.1 %collective-permute-start.1 = (bf16[192,2048]{1,0:T(8,128)(2,1)S(1)}, bf16[192,2048]{1,0:T(8,128)(2,1)S(1)}, u32[]{:S(2)}, u32[]{:S(2)}) collective-permute-start(bf16[192,2048]{1,0:T(8,128)(2,1)S(1)} %fusion.2.refs_0_), channel_id=1, source_target_pairs={{0,2},{1,3},{2,0},{3,1},{4,6},{5,7},{6,4},{7,5},{8,10},{9,11},{10,... | collective-permute-start | bytes 2359304 | tf_op jit(solution)/shard_map/ppermute | solution.py:504
  11.3 30.1 %collective-permute-start.3 = (bf16[192,2048]{1,0:T(8,128)(2,1)S(1)}, bf16[192,2048]{1,0:T(8,128)(2,1)S(1)}, u32[]{:S(2)}, u32[]{:S(2)}) collective-permute-start(bf16[192,2048]{1,0:T(8,128)(2,1)S(1)} %fusion.2.refs_0_), channel_id=1, source_target_pairs={{0,4},{1,5},{2,6},{3,7},{4,0},{5,1},{6,2},{7,3},{8,12},{9,13},{10,... | collective-permute-start | bytes 2359304 | tf_op jit(solution)/shard_map/ppermute | solution.py:504
  18.9 28.2 %collective-permute-start = (bf16[192,2048]{1,0:T(8,128)(2,1)S(1)}, bf16[192,2048]{1,0:T(8,128)(2,1)}, u32[]{:S(2)}, u32[]{:S(2)}) collective-permute-start(bf16[192,2048]{1,0:T(8,128)(2,1)S(1)} %fusion.2.refs_0_), channel_id=1, source_target_pairs={{0,1},{1,0},{2,3},{3,2},{4,5},{5,4},{6,7},{7,6},{8,9},{9,8},{10,11... | collective-permute-start | bytes 2359304 | tf_op jit(solution)/shard_map/ppermute | solution.py:504
  19.8 25.7 %collective-permute-start.32 = (bf16[512,512]{1,0:T(8,128)(2,1)}, bf16[512,512]{1,0:T(8,128)(2,1)}, u32[]{:S(2)}, u32[]{:S(2)}) collective-permute-start(bf16[512,512]{1,0:T(8,128)(2,1)} %pad_maximum_fusion.3.refs_0_), channel_id=1, source_target_pairs={{0,8},{1,9},{2,10},{3,11},{4,12},{5,13},{6,14},{7,15},{8,0},{9,1},... | collective-permute-start | bytes 1572872 | tf_op jit(solution)/shard_map/ppermute | solution.py:504
  23.5 23.5 %collective-permute-start.33 = (bf16[512,512]{1,0:T(8,128)(2,1)}, bf16[512,512]{1,0:T(8,128)(2,1)}, u32[]{:S(2)}, u32[]{:S(2)}) collective-permute-start(bf16[512,512]{1,0:T(8,128)(2,1)} %pad_maximum_fusion.3.refs_0_), channel_id=1, source_target_pairs={{8,16},{9,17},{10,18},{11,19},{12,20},{13,21},{14,22},{15,23},{16,... | collective-permute-start | bytes 1572872 | tf_op jit(solution)/shard_map/ppermute | solution.py:504
  25.0 15.0 %collective-permute-start.12 = (bf16[512,256]{1,0:T(8,128)(2,1)}, bf16[512,256]{1,0:T(8,128)(2,1)}, u32[]{:S(2)}, u32[]{:S(2)}) collective-permute-start(bf16[512,256]{1,0:T(8,128)(2,1)} %collective-permute-done.11.refs_12_), channel_id=1, source_target_pairs={{8,0},{9,1},{10,2},{11,3},{12,4},{13,5},{14,6},{15,7},{16,24},{17,... | collective-permute-start | bytes 786440 | tf_op jit(solution)/shard_map/ppermute | solution.py:504
  47.1 14.4 %collective-permute-start.2 = (bf16[192,2048]{1,0:T(8,128)(2,1)S(1)}, bf16[192,2048]{1,0:T(8,128)(2,1)}, u32[]{:S(2)}, u32[]{:S(2)}) collective-permute-start(bf16[192,2048]{1,0:T(8,128)(2,1)S(1)} %collective-permute-done.1.refs_2_), channel_id=1, source_target_pairs={{0,1},{1,0},{2,3},{3,2},{4,5},{5,4},{6,7},{7,6},{8,9},{9,8},{10,11... | collective-permute-start | bytes 2359304 | tf_op jit(solution)/shard_map/ppermute | solution.py:504
  47.2 15.8 %collective-permute-start.4 = (bf16[192,2048]{1,0:T(8,128)(2,1)S(1)}, bf16[192,2048]{1,0:T(8,128)(2,1)S(1)}, u32[]{:S(2)}, u32[]{:S(2)}) collective-permute-start(bf16[192,2048]{1,0:T(8,128)(2,1)S(1)} %collective-permute-done.3.refs_4_), channel_id=1, source_target_pairs={{0,1},{1,0},{2,3},{3,2},{4,5},{5,4},{6,7},{7,6},{8,9},{9,8},{10,11... | collective-permute-start | bytes 2359304 | tf_op jit(solution)/shard_map/ppermute | solution.py:504
  57.7 32.0 %collective-permute-start.34 = (bf16[512,512]{1,0:T(8,128)(2,1)}, bf16[512,512]{1,0:T(8,128)(2,1)S(1)}, u32[]{:S(2)}, u32[]{:S(2)}) collective-permute-start(bf16[512,512]{1,0:T(8,128)(2,1)} %collective-permute-done.33.refs_2_), channel_id=1, source_target_pairs={{8,0},{9,1},{10,2},{11,3},{12,4},{13,5},{14,6},{15,7},{16,24},{17,... | collective-permute-start | bytes 1572872 | tf_op jit(solution)/shard_map/ppermute | solution.py:504
  59.0 40.5 %collective-permute-start.36 = (bf16[512,512]{1,0:T(8,128)(2,1)}, bf16[512,512]{1,0:T(8,128)(2,1)S(1)}, u32[]{:S(2)}, u32[]{:S(2)}) collective-permute-start(bf16[512,512]{1,0:T(8,128)(2,1)} %collective-permute-done.35.refs_4_), channel_id=1, source_target_pairs={{8,0},{9,1},{10,2},{11,3},{12,4},{13,5},{14,6},{15,7},{16,24},{17,... | collective-permute-start | bytes 1572872 | tf_op jit(solution)/shard_map/ppermute | solution.py:504
  61.0 48.1 %collective-permute-start.37 = (bf16[768,128]{1,0:T(8,128)(2,1)}, bf16[768,128]{1,0:T(8,128)(2,1)S(1)}, u32[]{:S(2)}, u32[]{:S(2)}) collective-permute-start(bf16[768,128]{1,0:T(8,128)(2,1)} %dynamic-slice_convert_fusion), channel_id=1, source_target_pairs={{0,4},{1,5},{2,6},{3,7},{4,0},{5,1},{6,2},{7,3},{8,12},{9,13},{10,... | collective-permute-start | bytes 589832 | tf_op jit(solution)/shard_map/ppermute | solution.py:504
  61.5 55.2 %collective-permute-start.21 = (bf16[256,512]{1,0:T(8,128)(2,1)S(1)}, bf16[256,512]{1,0:T(8,128)(2,1)S(1)}, u32[]{:S(2)}, u32[]{:S(2)}) collective-permute-start(bf16[256,512]{1,0:T(8,128)(2,1)S(1)} %pad_maximum_fusion.5), channel_id=1, source_target_pairs={{0,4},{1,5},{2,6},{3,7},{4,0},{5,1},{6,2},{7,3},{8,12},{9,13},{10,... | collective-permute-start | bytes 786440 | tf_op jit(solution)/shard_map/ppermute | solution.py:504
  72.1 13.4 %collective-permute-start.15 = (bf16[32,128]{1,0:T(8,128)(2,1)S(1)}, bf16[32,128]{1,0:T(8,128)(2,1)S(1)}, u32[]{:S(2)}, u32[]{:S(2)}) collective-permute-start(bf16[32,128]{1,0:T(8,128)(2,1)S(1)} %slice.11), channel_id=1, source_target_pairs={{0,8},{1,9},{2,10},{3,11},{4,12},{5,13},{6,14},{7,15},{8,16},{9,17... | collective-permute-start | bytes 24584 | tf_op jit(solution)/shard_map/ppermute | solution.py:504
  85.4 33.1 %collective-permute-start.27 = (bf16[256,512]{1,0:T(8,128)(2,1)S(1)}, bf16[256,512]{1,0:T(8,128)(2,1)S(1)}, u32[]{:S(2)}, u32[]{:S(2)}) collective-permute-start(bf16[256,512]{1,0:T(8,128)(2,1)S(1)} %pad_maximum_fusion.6), channel_id=1, source_target_pairs={{0,0},{1,8},{2,16},{3,24},{4,4},{5,12},{6,20},{7,28},{8,1},{9,9},{... | collective-permute-start | bytes 786440 | tf_op jit(solution)/shard_map/ppermute | solution.py:504
  89.7 42.9 %collective-permute-start.16 = (bf16[1552,128]{1,0:T(8,128)(2,1)}, bf16[1552,128]{1,0:T(8,128)(2,1)S(1)}, u32[]{:S(2)}, u32[]{:S(2)}) collective-permute-start(bf16[1552,128]{1,0:T(8,128)(2,1)} %shard_map.181.refs_0_), channel_id=1, source_target_pairs={{0,2},{1,3},{2,0},{3,1},{4,6},{5,7},{6,4},{7,5},{8,10},{9,11},{10,... | collective-permute-start | bytes 1191944 | tf_op jit(solution)/shard_map/ppermute | solution.py:504
  99.5 33.7 %collective-permute-start.17 = (bf16[1552,128]{1,0:T(8,128)(2,1)}, bf16[1552,128]{1,0:T(8,128)(2,1)S(1)}, u32[]{:S(2)}, u32[]{:S(2)}) collective-permute-start(bf16[1552,128]{1,0:T(8,128)(2,1)} %shard_map.181.refs_0_), channel_id=1, source_target_pairs={{0,4},{1,5},{2,6},{3,7},{4,0},{5,1},{6,2},{7,3},{8,12},{9,13},{10,... | collective-permute-start | bytes 1191944 | tf_op jit(solution)/shard_map/ppermute | solution.py:504
  109.0 25.0 %collective-permute-start.18 = (bf16[1552,128]{1,0:T(8,128)(2,1)}, bf16[1552,128]{1,0:T(8,128)(2,1)S(1)}, u32[]{:S(2)}, u32[]{:S(2)}) collective-permute-start(bf16[1552,128]{1,0:T(8,128)(2,1)} %shard_map.181.refs_0_), channel_id=1, source_target_pairs={{0,6},{1,7},{2,4},{3,5},{4,2},{5,3},{6,0},{7,1},{8,14},{9,15},{10,... | collective-permute-start | bytes 1191944 | tf_op jit(solution)/shard_map/ppermute | solution.py:504
  127.1 27.2 %collective-permute-start.22 = (bf16[512,512]{1,0:T(8,128)(2,1)S(1)}, bf16[512,512]{1,0:T(8,128)(2,1)S(1)}, u32[]{:S(2)}, u32[]{:S(2)}) collective-permute-start(bf16[512,512]{1,0:T(8,128)(2,1)S(1)} %pad_maximum_fusion.2.refs_0_), channel_id=1, source_target_pairs={{0,8},{1,9},{2,10},{3,11},{4,12},{5,13},{6,14},{7,15},{8,0},{9,1},... | collective-permute-start | bytes 1572872 | tf_op jit(solution)/shard_map/ppermute | solution.py:504
  129.2 24.5 %collective-permute-start.28 = (bf16[256,512]{1,0:T(8,128)(2,1)S(1)}, bf16[256,512]{1,0:T(8,128)(2,1)S(1)}, u32[]{:S(2)}, u32[]{:S(2)}) collective-permute-start(bf16[256,512]{1,0:T(8,128)(2,1)S(1)} %collective-permute-done.27.refs_6_), channel_id=1, source_target_pairs={{0,8},{1,9},{2,10},{3,11},{4,12},{5,13},{6,14},{7,15},{8,0},{9,1},... | collective-permute-start | bytes 786440 | tf_op jit(solution)/shard_map/ppermute | solution.py:504
  132.6 12.2 %collective-permute-start.41 = (bf16[1536,128]{1,0:T(8,128)(2,1)}, bf16[1536,128]{1,0:T(8,128)(2,1)S(1)}, u32[]{:S(2)}, u32[]{:S(2)}) collective-permute-start(bf16[1536,128]{1,0:T(8,128)(2,1)} %finish.1.refs_10_), channel_id=1, source_target_pairs={{0,2},{1,3},{2,0},{3,1},{4,6},{5,7},{6,4},{7,5},{8,10},{9,11},{10,... | collective-permute-start | bytes 1179656 | tf_op jit(solution)/shard_map/ppermute | solution.py:504
  133.2 16.7 %collective-permute-start.42 = (bf16[1536,128]{1,0:T(8,128)(2,1)}, bf16[1536,128]{1,0:T(8,128)(2,1)S(1)}, u32[]{:S(2)}, u32[]{:S(2)}) collective-permute-start(bf16[1536,128]{1,0:T(8,128)(2,1)} %finish.1.refs_10_), channel_id=1, source_target_pairs={{0,4},{1,5},{2,6},{3,7},{4,0},{5,1},{6,2},{7,3},{8,12},{9,13},{10,... | collective-permute-start | bytes 1179656 | tf_op jit(solution)/shard_map/ppermute | solution.py:504
  134.0 15.9 %collective-permute-start.43 = (bf16[1536,128]{1,0:T(8,128)(2,1)}, bf16[1536,128]{1,0:T(8,128)(2,1)S(1)}, u32[]{:S(2)}, u32[]{:S(2)}) collective-permute-start(bf16[1536,128]{1,0:T(8,128)(2,1)} %finish.1.refs_10_), channel_id=1, source_target_pairs={{0,6},{1,7},{2,4},{3,5},{4,2},{5,3},{6,0},{7,1},{8,14},{9,15},{10,... | collective-permute-start | bytes 1179656 | tf_op jit(solution)/shard_map/ppermute | solution.py:504
  144.8 25.1 %collective-permute-start.20 = (bf16[4656,128]{1,0:T(8,128)(2,1)S(1)}, bf16[4656,128]{1,0:T(8,128)(2,1)S(1)}, u32[]{:S(2)}, u32[]{:S(2)}) collective-permute-start(bf16[4656,128]{1,0:T(8,128)(2,1)S(1)} %pad_maximum_fusion), channel_id=1, source_target_pairs={{0,1},{1,0},{2,3},{3,2},{4,5},{5,4},{6,7},{7,6},{8,9},{9,8},{10,11... | collective-permute-start | bytes 3575816 | tf_op jit(solution)/shard_map/ppermute | solution.py:504
  150.0 58.0 %collective-permute-start.45 = (bf16[4608,128]{1,0:T(8,128)(2,1)S(1)}, bf16[4608,128]{1,0:T(8,128)(2,1)S(1)}, u32[]{:S(2)}, u32[]{:S(2)}) collective-permute-start(bf16[4608,128]{1,0:T(8,128)(2,1)S(1)} %pad_maximum_fusion.1), channel_id=1, source_target_pairs={{0,1},{1,0},{2,3},{3,2},{4,5},{5,4},{6,7},{7,6},{8,9},{9,8},{10,11... | collective-permute-start | bytes 3538952 | tf_op jit(solution)/shard_map/ppermute | solution.py:504
  150.1 16.4 %collective-permute-start.29 = (bf16[256,512]{1,0:T(8,128)(2,1)S(1)}, bf16[256,512]{1,0:T(8,128)(2,1)S(1)}, u32[]{:S(2)}, u32[]{:S(2)}) collective-permute-start(bf16[256,512]{1,0:T(8,128)(2,1)S(1)} %collective-permute-done.27.refs_6_), channel_id=1, source_target_pairs={{0,16},{1,17},{2,18},{3,19},{4,20},{5,21},{6,22},{7,23},{8,24},{9,... | collective-permute-start | bytes 786440 | tf_op jit(solution)/shard_map/ppermute | solution.py:504
  153.7 12.8 %collective-permute-start.23 = (bf16[512,512]{1,0:T(8,128)(2,1)S(1)}, bf16[512,512]{1,0:T(8,128)(2,1)S(1)}, u32[]{:S(2)}, u32[]{:S(2)}) collective-permute-start(bf16[512,512]{1,0:T(8,128)(2,1)S(1)} %pad_maximum_fusion.2.refs_0_), channel_id=1, source_target_pairs={{8,16},{9,17},{10,18},{11,19},{12,20},{13,21},{14,22},{15,23},{16,... | collective-permute-start | bytes 1572872 | tf_op jit(solution)/shard_map/ppermute | solution.py:504
  154.4 13.4 %collective-permute-start.25 = (bf16[512,512]{1,0:T(8,128)(2,1)S(1)}, bf16[512,512]{1,0:T(8,128)(2,1)S(1)}, u32[]{:S(2)}, u32[]{:S(2)}) collective-permute-start(bf16[512,512]{1,0:T(8,128)(2,1)S(1)} %collective-permute-done.22.refs_1_), channel_id=1, source_target_pairs={{8,16},{9,17},{10,18},{11,19},{12,20},{13,21},{14,22},{15,23},{16,... | collective-permute-start | bytes 1572872 | tf_op jit(solution)/shard_map/ppermute | solution.py:504
  166.5 30.3 %collective-permute-start.24 = (bf16[512,512]{1,0:T(8,128)(2,1)S(1)}, bf16[512,512]{1,0:T(8,128)(2,1)S(1)}, u32[]{:S(2)}, u32[]{:S(2)}) collective-permute-start(bf16[512,512]{1,0:T(8,128)(2,1)S(1)} %collective-permute-done.23.refs_2_), channel_id=1, source_target_pairs={{8,0},{9,1},{10,2},{11,3},{12,4},{13,5},{14,6},{15,7},{16,24},{17,... | collective-permute-start | bytes 1572872 | tf_op jit(solution)/shard_map/ppermute | solution.py:504
  167.8 40.3 %collective-permute-start.26 = (bf16[512,512]{1,0:T(8,128)(2,1)S(1)}, bf16[512,512]{1,0:T(8,128)(2,1)S(1)}, u32[]{:S(2)}, u32[]{:S(2)}) collective-permute-start(bf16[512,512]{1,0:T(8,128)(2,1)S(1)} %collective-permute-done.25.refs_4_), channel_id=1, source_target_pairs={{8,0},{9,1},{10,2},{11,3},{12,4},{13,5},{14,6},{15,7},{16,24},{17,... | collective-permute-start | bytes 1572872 | tf_op jit(solution)/shard_map/ppermute | solution.py:504
  169.3 38.7 %collective-permute-start.44 = (bf16[1536,128]{1,0:T(8,128)(2,1)S(1)}, bf16[1536,128]{1,0:T(8,128)(2,1)S(1)}, u32[]{:S(2)}, u32[]{:S(2)}) collective-permute-start(bf16[1536,128]{1,0:T(8,128)(2,1)S(1)} %copy-done.15), channel_id=1, source_target_pairs={{0,1},{1,0},{2,3},{3,2},{4,5},{5,4},{6,7},{7,6},{8,9},{9,8},{10,11... | collective-permute-start | bytes 1179656 | tf_op jit(solution)/shard_map/ppermute | solution.py:504
  171.1 10.7 %collective-permute-start.30 = (bf16[256,512]{1,0:T(8,128)(2,1)S(1)}, bf16[256,512]{1,0:T(8,128)(2,1)}, u32[]{:S(2)}, u32[]{:S(2)}) collective-permute-start(bf16[256,512]{1,0:T(8,128)(2,1)S(1)} %collective-permute-done.27.refs_6_), channel_id=1, source_target_pairs={{0,24},{1,25},{2,26},{3,27},{4,28},{5,29},{6,30},{7,31},{8,16},{9,... | collective-permute-start | bytes 786440 | tf_op jit(solution)/shard_map/ppermute | solution.py:504
  217.7 10.6 %collective-permute-start.46 = (bf16[768,256]{1,0:T(8,128)(2,1)}, bf16[768,256]{1,0:T(8,128)(2,1)S(1)}, u32[]{:S(2)}, u32[]{:S(2)}) collective-permute-start(bf16[768,256]{1,0:T(8,128)(2,1)} %combine.2), channel_id=1, source_target_pairs={{0,4},{1,5},{2,6},{3,7},{4,0},{5,1},{6,2},{7,3},{8,12},{9,13},{10,... | collective-permute-start | bytes 1179656 | tf_op jit(solution)/shard_map/ppermute | solution.py:504
  (59 other events, 733.5 us)

commit v2 on v1

--- a/solution.py
+++ b/solution.py
@@ -66,7 +66,7 @@
 
 
 def params():
-    return pltpu.CompilerParams(vmem_limit_bytes=56 * 1024 * 1024)
+    return pltpu.CompilerParams(vmem_limit_bytes=20 * 1024 * 1024)
 
 
 def cost(flops, moved):
@@ -177,7 +177,7 @@
         carry = (jnp.zeros((HEAD, HEAD), f32), jnp.zeros((1, HEAD), f32))
         for side in range(n_decays):
             carry = lax.fori_loop(
-                0, half // CHUNK, functools.partial(step, side), carry, unroll=3
+                0, half // CHUNK, functools.partial(step, side), carry, unroll=6
             )
         state, total = carry
         decay = jnp.exp(total)
@@ -204,7 +204,7 @@
 
 
 def heads(rows, depth, weight_copies, n_weights):
-    size = rows // 4
+    size = rows // 2
 
     def body(scalars, tokens, *refs):
         weights, (raw_out, outgate, weight_v, semaphores) = refs[:n_weights], refs[n_weights:]
@@ -363,7 +363,7 @@
 def combine(rows, start, lane, depth, channels, width, wide, copies, counts):
     gate_copies, out_copies, rec_copies = copies
     n_weights, n_outs, n_rec = counts
-    blocks = 3 if rows % (3 * 128) == 0 else 2
+    blocks = 2
     size = rows // blocks
 
     def body(scalars, tokens, conv, *refs):
@@ -440,9 +440,9 @@
         out_shape=jax.ShapeDtypeStruct((rows, 2 * width), bf16),
         grid_spec=pltpu.PrefetchScalarGridSpec(
             num_scalar_prefetch=1,
-            grid=(2,),
-            in_specs=[pl.BlockSpec((rows // 2, width), lambda i, scalars: (i, 0)), HBM],
-            out_specs=pl.BlockSpec((rows // 2, width), lambda i, scalars: (i, 1 - scalars[1])),
+            grid=(1,),
+            in_specs=[pl.BlockSpec((rows, width), lambda i, scalars: (i, 0)), HBM],
+            out_specs=pl.BlockSpec((rows, width), lambda i, scalars: (i, 1 - scalars[1])),
         ),
         input_output_aliases={2: 0},
         compiler_params=params(),

time: 232 us -> 218 us (0.940)
  Pallas kernels: 54.4 us -> 39 us
  local copies, waits for them, and re-layouts: 17.4 us -> 8.35 us
  waiting for transfers between devices: 75.2 us -> 83.3 us
  starting transfers between devices: 78.7 us -> 81.8 us
    ppermute x47, waiting for transfers between devices: 75.2 us -> 83.3 us  [send(): return lax.ppermute(value, AXES, pairs)]
    unnamed x88 -> x36, local copies, waits for them, and re-layouts: 5.9 us -> 1.97 us
    pallas_call x1, Pallas kernels: 8.67 us -> 5.47 us  [local(): heads(rows, depth, rows_of(sub * q, inner), len(weights_b))]
    ppermute x47, starting transfers between devices: 78.7 us -> 81.8 us  [send(): return lax.ppermute(value, AXES, pairs)]
    pallas_call x2, Pallas kernels: 15.5 us -> 12.8 us  [final_rows(): combine(half, lambda z, y, own: (y ^ keep) * half, lambda z, y, own: y if...]
    pallas_call x1, Pallas kernels: 7.22 us -> 4.82 us  [local(): activate(rows, channels, groups, tail_copies, len(conv_arrays))]
    pallas_call x1, Pallas kernels: 6.86 us -> 4.5 us  [local(): recurrence(rows, half, q)]
  transfers between devices with their start and end apart: 47 -> 47, of which waited for: 15 -> 14; matrix products, arithmetic and copies ran while one was open for 7% -> 5% of each run, Pallas kernels for 19% -> 15%
where the time goes in v2:
time: 218 us
  waiting for transfers between devices  83.3 us (38%)
  starting transfers between devices  81.8 us (38%)
  Pallas kernels  39 us (18%)
  local copies, waits for them, and re-layouts  8.35 us (4%)
  other arithmetic  4.6 us (2%)
    ppermute x47, waiting for transfers between devices, send(): return lax.ppermute(value, AXES, pairs)  83.3 us
    ppermute x47, starting transfers between devices, send(): return lax.ppermute(value, AXES, pairs)  81.8 us
    pallas_call x2, Pallas kernels, final_rows(): combine(half, lambda z, y, own: (y ^ keep) * half, lambda z, y, own: y if...  12.8 us
    pallas_call x1, Pallas kernels, local(): project(rows, depth, token_groups, len(token_arrays), rows_of(sub * q, in...  7.1 us
    pallas_call x1, Pallas kernels, local(): heads(rows, depth, rows_of(sub * q, inner), len(weights_b))  5.47 us
    pallas_call x1, Pallas kernels, local(): activate(rows, channels, groups, tail_copies, len(conv_arrays))  4.82 us
    pallas_call x1, Pallas kernels, local(): recurrence(rows, half, q)  4.5 us
  transfers between devices with their start and end apart: 47, of which 14 were waited for; matrix products, arithmetic and copies ran while one was open for 5% of the time, Pallas kernels for 15%

profile of v2, /device:TPU:0, one launch (start us, length us, event | category | flops | bytes accessed | tf_op | source)
XLA Modules:
  0.0 217.6 jit_solution(9022840763506807327)
XLA Ops:
  1.2 3.1 %collective-permute-start.9 = (bf16[256,256]{1,0:T(8,128)(2,1)S(1)}, bf16[256,256]{1,0:T(8,128)(2,1)S(1)}, u32[]{:S(2)}, u32[]{:S(2)}) collective-permute-start(bf16[256,256]{1,0:T(8,128)(2,1)S(1)} %pad_maximum_fusion.8), channel_id=1, source_target_pairs={{0,4},{1,5},{2,6},{3,7},{4,0},{5,1},{6,2},{7,3},{8,12},{9,13},{10,... | collective-permute-start | bytes 393224 | tf_op jit(solution)/shard_map/ppermute | solution.py:504
  7.8 1.9 collective-permute-start.10
  9.7 1.6 collective-permute-start.31
  13.1 2.2 collective-permute-done.10.refs_11_
  16.0 2.9 %collective-permute-done.31 = bf16[256,512]{1,0:T(8,128)(2,1)S(1)} collective-permute-done((bf16[256,512]{1,0:T(8,128)(2,1)S(1)}, bf16[256,512]{1,0:T(8,128)(2,1)S(1)}, u32[]{:S(2)}, u32[]{:S(2)}) %collective-permute-start.31) | collective-permute-done | bytes 262176 | tf_op jit(solution)/shard_map/ppermute | solution.py:504
  19.8 3.7 %collective-permute-start.32 = (bf16[512,512]{1,0:T(8,128)(2,1)}, bf16[512,512]{1,0:T(8,128)(2,1)}, u32[]{:S(2)}, u32[]{:S(2)}) collective-permute-start(bf16[512,512]{1,0:T(8,128)(2,1)} %pad_maximum_fusion.3.refs_0_), channel_id=1, source_target_pairs={{0,8},{1,9},{2,10},{3,11},{4,12},{5,13},{6,14},{7,15},{8,0},{9,1},... | collective-permute-start | bytes 1572872 | tf_op jit(solution)/shard_map/ppermute | solution.py:504
  27.1 13.0 %collective-permute-done.12.refs_13_ = bf16[512,256]{1,0:T(8,128)(2,1)} collective-permute-done((bf16[512,256]{1,0:T(8,128)(2,1)}, bf16[512,256]{1,0:T(8,128)(2,1)}, u32[]{:S(2)}, u32[]{:S(2)}) %collective-permute-start.12) | collective-permute-done | bytes 262176 | tf_op jit(solution)/shard_map/ppermute | solution.py:504
  41.3 1.6 collective-permute-start.5
  42.9 1.8 constant_dynamic-slice_fusion.11
  51.4 3.1 %collective-permute-done.7.refs_8_ = bf16[96,2048]{1,0:T(8,128)(2,1)} collective-permute-done((bf16[96,2048]{1,0:T(8,128)(2,1)}, bf16[96,2048]{1,0:T(8,128)(2,1)}, u32[]{:S(2)}, u32[]{:S(2)}) %collective-permute-start.7) | collective-permute-done | bytes 393248 | tf_op jit(solution)/shard_map/ppermute | solution.py:504
  62.3 7.1 %project.1 = (bf16[1536,128]{1,0:T(8,128)(2,1)S(1)}, bf16[1536,2048]{1,0:T(8,128)(2,1)S(1)}) custom-call(s32[3]{0:T(128)S(1)} %pad_add_fusion.scalars, bf16[192,2048]{1,0:T(8,128)(2,1)S(1)} %fusion.2.refs_0_, bf16[192,2048]{1,0:T(8,128)(2,1)} %collective-permute-done.refs_1_, bf16[192,2048]{1,0:T(8,128)(2,1)S(1)} %collective-permute-done.1.refs_2_, ...), custom_call_target="tpu_custom_call" | custom-call | flops 1610612736 | bytes 12582912 | tf_op jit(solution)/shard_map/project/pallas_call | solution.py:647
  69.4 14.8 %collective-permute-start.15 = (bf16[32,128]{1,0:T(8,128)(2,1)S(1)}, bf16[32,128]{1,0:T(8,128)(2,1)S(1)}, u32[]{:S(2)}, u32[]{:S(2)}) collective-permute-start(bf16[32,128]{1,0:T(8,128)(2,1)S(1)} %slice.11), channel_id=1, source_target_pairs={{0,8},{1,9},{2,10},{3,11},{4,12},{5,13},{6,14},{7,15},{8,16},{9,17... | collective-permute-start | bytes 24584 | tf_op jit(solution)/shard_map/ppermute | solution.py:504
  86.3 1.8 shard_map.181.refs_0_
  88.1 10.3 %collective-permute-start.16 = (bf16[1552,128]{1,0:T(8,128)(2,1)S(1)}, bf16[1552,128]{1,0:T(8,128)(2,1)S(1)}, u32[]{:S(2)}, u32[]{:S(2)}) collective-permute-start(bf16[1552,128]{1,0:T(8,128)(2,1)S(1)} %shard_map.181.refs_0_), channel_id=1, source_target_pairs={{0,2},{1,3},{2,0},{3,1},{4,6},{5,7},{6,4},{7,5},{8,10},{9,11},{10,... | collective-permute-start | bytes 1191944 | tf_op jit(solution)/shard_map/ppermute | solution.py:504
  98.9 5.5 %heads.1 = (bf16[1536,384]{1,0:T(8,128)(2,1)S(1)}, bf16[1536,128]{1,0:T(8,128)(2,1)S(1)}) custom-call(s32[3]{0:T(128)S(1)} %pad_add_fusion.scalars, bf16[1536,2048]{1,0:T(8,128)(2,1)S(1)} %get-tuple-element.12.tokens, bf16[512,512]{1,0:T(8,128)(2,1)} %pad_maximum_fusion.3.refs_0_, bf16[512,512]{1,0:T(8,128)(2,1)} %collective-permute-done.32.refs_1_, ...), custom_call_target="tpu_custom_call" | custom-call | flops 3221225472 | bytes 6291456 | tf_op jit(solution)/shard_map/heads/pallas_call | solution.py:664
  105.5 4.5 %recurrence.1 = (f32[1536,128]{1,0:T(8,128)S(1)}, bf16[1536,128]{1,0:T(8,128)(2,1)S(1)}, bf16[144,128]{1,0:T(8,128)(2,1)S(1)}) custom-call(s32[3]{0:T(128)S(1)} %pad_add_fusion.scalars, bf16[1536,384]{1,0:T(8,128)(2,1)S(1)} %get-tuple-element.14.raw, f32[1,128]{1,0:T(1,128)S(1)} %subtract_bitcast_fusion.rate, ...), custom_call_target="tpu_custom_call" | custom-call | flops 2516582400 | bytes 3145728 | tf_op jit(solution)/shard_map/recurrence/pallas_call | solution.py:667
  111.4 5.5 %collective-permute-start.39 = (bf16[144,128]{1,0:T(8,128)(2,1)S(1)}, bf16[144,128]{1,0:T(8,128)(2,1)S(1)}, u32[]{:S(2)}, u32[]{:S(2)}) collective-permute-start(bf16[144,128]{1,0:T(8,128)(2,1)S(1)} %get-tuple-element.18), channel_id=1, source_target_pairs={{0,16},{1,17},{2,18},{3,19},{4,20},{5,21},{6,22},{7,23},{8,24},{9,... | collective-permute-start | bytes 110600 | tf_op jit(solution)/shard_map/ppermute | solution.py:504
  116.9 3.3 %collective-permute-start.40 = (bf16[144,128]{1,0:T(8,128)(2,1)S(1)}, bf16[144,128]{1,0:T(8,128)(2,1)S(1)}, u32[]{:S(2)}, u32[]{:S(2)}) collective-permute-start(bf16[144,128]{1,0:T(8,128)(2,1)S(1)} %get-tuple-element.18), channel_id=1, source_target_pairs={{0,24},{1,25},{2,26},{3,27},{4,28},{5,29},{6,30},{7,31}} | collective-permute-start | bytes 110600 | tf_op jit(solution)/shard_map/ppermute | solution.py:504
  120.4 1.7 collective-permute-done.40.refs_2_
  124.6 2.5 %collective-permute-start.43 = (bf16[1536,128]{1,0:T(8,128)(2,1)S(1)}, bf16[1536,128]{1,0:T(8,128)(2,1)S(1)}, u32[]{:S(2)}, u32[]{:S(2)}) collective-permute-start(bf16[1536,128]{1,0:T(8,128)(2,1)S(1)} %finish.1.refs_10_), channel_id=1, source_target_pairs={{0,6},{1,7},{2,4},{3,5},{4,2},{5,3},{6,0},{7,1},{8,14},{9,15},{10,... | collective-permute-start | bytes 1179656 | tf_op jit(solution)/shard_map/ppermute | solution.py:504
  127.2 8.4 %collective-permute-done.41.refs_11_ = bf16[1536,128]{1,0:T(8,128)(2,1)S(1)} collective-permute-done((bf16[1536,128]{1,0:T(8,128)(2,1)S(1)}, bf16[1536,128]{1,0:T(8,128)(2,1)S(1)}, u32[]{:S(2)}, u32[]{:S(2)}) %collective-permute-start.41) | collective-permute-done | bytes 393248 | tf_op jit(solution)/shard_map/ppermute | solution.py:504
  135.6 5.9 %collective-permute-done.42.refs_12_ = bf16[1536,128]{1,0:T(8,128)(2,1)S(1)} collective-permute-done((bf16[1536,128]{1,0:T(8,128)(2,1)S(1)}, bf16[1536,128]{1,0:T(8,128)(2,1)S(1)}, u32[]{:S(2)}, u32[]{:S(2)}) %collective-permute-start.42) | collective-permute-done | bytes 393248 | tf_op jit(solution)/shard_map/ppermute | solution.py:504
  141.6 3.7 %collective-permute-start.29 = (bf16[256,512]{1,0:T(8,128)(2,1)S(1)}, bf16[256,512]{1,0:T(8,128)(2,1)S(1)}, u32[]{:S(2)}, u32[]{:S(2)}) collective-permute-start(bf16[256,512]{1,0:T(8,128)(2,1)S(1)} %collective-permute-done.27.refs_6_), channel_id=1, source_target_pairs={{0,16},{1,17},{2,18},{3,19},{4,20},{5,21},{6,22},{7,23},{8,24},{9,... | collective-permute-start | bytes 786440 | tf_op jit(solution)/shard_map/ppermute | solution.py:504
  146.7 10.8 %collective-permute-done.29.refs_8_ = bf16[256,512]{1,0:T(8,128)(2,1)S(1)} collective-permute-done((bf16[256,512]{1,0:T(8,128)(2,1)S(1)}, bf16[256,512]{1,0:T(8,128)(2,1)S(1)}, u32[]{:S(2)}, u32[]{:S(2)}) %collective-permute-start.29) | collective-permute-done | bytes 262176 | tf_op jit(solution)/shard_map/ppermute | solution.py:504
  161.0 3.2 %collective-permute-start.30 = (bf16[256,512]{1,0:T(8,128)(2,1)S(1)}, bf16[256,512]{1,0:T(8,128)(2,1)S(1)}, u32[]{:S(2)}, u32[]{:S(2)}) collective-permute-start(bf16[256,512]{1,0:T(8,128)(2,1)S(1)} %collective-permute-done.27.refs_6_), channel_id=1, source_target_pairs={{0,24},{1,25},{2,26},{3,27},{4,28},{5,29},{6,30},{7,31},{8,16},{9,... | collective-permute-start | bytes 786440 | tf_op jit(solution)/shard_map/ppermute | solution.py:504
  164.1 4.8 %activate.1.conv = bf16[1536,1024]{1,0:T(8,128)(2,1)S(1)} custom-call(s32[3]{0:T(128)S(1)} %pad_add_fusion.scalars, bf16[1552,128]{1,0:T(8,128)(2,1)S(1)} %shard_map.181.refs_0_, bf16[1552,128]{1,0:T(8,128)(2,1)S(1)} %collective-permute-done.16.refs_1_, bf16[1552,128]{1,0:T(8,128)(2,1)S(1)} %collective-permute-done.17.refs_2_, ...), custom_call_target="tpu_custom_call" | custom-call | flops 3145728000 | bytes 6291456 | tf_op jit(solution)/shard_map/activate/pallas_call | solution.py:719
  169.0 2.2 %collective-permute-done.30.refs_9_ = bf16[256,512]{1,0:T(8,128)(2,1)S(1)} collective-permute-done((bf16[256,512]{1,0:T(8,128)(2,1)S(1)}, bf16[256,512]{1,0:T(8,128)(2,1)S(1)}, u32[]{:S(2)}, u32[]{:S(2)}) %collective-permute-start.30) | collective-permute-done | bytes 262176 | tf_op jit(solution)/shard_map/ppermute | solution.py:504
  171.2 17.3 %collective-permute-done.24.refs_3_ = bf16[512,512]{1,0:T(8,128)(2,1)S(1)} collective-permute-done((bf16[512,512]{1,0:T(8,128)(2,1)S(1)}, bf16[512,512]{1,0:T(8,128)(2,1)S(1)}, u32[]{:S(2)}, u32[]{:S(2)}) %collective-permute-start.24) | collective-permute-done | bytes 524320 | tf_op jit(solution)/shard_map/ppermute | solution.py:504
  188.4 11.2 %collective-permute-done.26.refs_5_ = bf16[512,512]{1,0:T(8,128)(2,1)S(1)} collective-permute-done((bf16[512,512]{1,0:T(8,128)(2,1)S(1)}, bf16[512,512]{1,0:T(8,128)(2,1)S(1)}, u32[]{:S(2)}, u32[]{:S(2)}) %collective-permute-start.26) | collective-permute-done | bytes 524320 | tf_op jit(solution)/shard_map/ppermute | solution.py:504
  199.7 6.0 %combine.2 = bf16[768,256]{1,0:T(8,128)(2,1)S(1)} custom-call(s32[3]{0:T(128)S(1)} %pad_add_fusion.scalars, bf16[1536,2048]{1,0:T(8,128)(2,1)S(1)} %get-tuple-element.12.tokens, bf16[1536,1024]{1,0:T(8,128)(2,1)S(1)} %activate.1.conv, bf16[512,512]{1,0:T(8,128)(2,1)S(1)} %pad_maximum_fusion.2.refs_0_, bf16[512,512]{1,0:T(8,128)(2,1)S(1)} %collective-permute-done.22.refs_1_, ...), custom_call_target="tpu_custom_call" | custom-call | flops 2415919104 | bytes 6291456 | tf_op jit(solution)/shard_map/combine/pallas_call | solution.py:736
  206.2 6.9 %combine.3.mine = bf16[768,512]{1,0:T(8,128)(2,1)} custom-call(s32[3]{0:T(128)S(1)} %pad_add_fusion.scalars, bf16[1536,2048]{1,0:T(8,128)(2,1)S(1)} %get-tuple-element.12.tokens, bf16[1536,1024]{1,0:T(8,128)(2,1)S(1)} %activate.1.conv, bf16[512,512]{1,0:T(8,128)(2,1)S(1)} %pad_maximum_fusion.2.refs_0_, bf16[512,512]{1,0:T(8,128)(2,1)S(1)} %collective-permute-done.22.refs_1_, ...), custom_call_target="tpu_custom_call" | custom-call | flops 2415919104 | bytes 6291456 | tf_op jit(solution)/shard_map/combine/pallas_call | solution.py:736
  213.1 3.1 %collective-permute-done.46.theirs = bf16[768,256]{1,0:T(8,128)(2,1)S(1)} collective-permute-done((bf16[768,256]{1,0:T(8,128)(2,1)S(1)}, bf16[768,256]{1,0:T(8,128)(2,1)S(1)}, u32[]{:S(2)}, u32[]{:S(2)}) %collective-permute-start.46) | collective-permute-done | bytes 393248 | tf_op jit(solution)/shard_map/ppermute | solution.py:504
  (135 shorter events, 41.8 us)
Async XLA Ops:
  5.9 19.1 %collective-permute-start.1 = (bf16[192,2048]{1,0:T(8,128)(2,1)S(1)}, bf16[192,2048]{1,0:T(8,128)(2,1)S(1)}, u32[]{:S(2)}, u32[]{:S(2)}) collective-permute-start(bf16[192,2048]{1,0:T(8,128)(2,1)S(1)} %fusion.2.refs_0_), channel_id=1, source_target_pairs={{0,2},{1,3},{2,0},{3,1},{4,6},{5,7},{6,4},{7,5},{8,10},{9,11},{10,... | collective-permute-start | bytes 2359304 | tf_op jit(solution)/shard_map/ppermute | solution.py:504
  11.3 30.1 %collective-permute-start.3 = (bf16[192,2048]{1,0:T(8,128)(2,1)S(1)}, bf16[192,2048]{1,0:T(8,128)(2,1)S(1)}, u32[]{:S(2)}, u32[]{:S(2)}) collective-permute-start(bf16[192,2048]{1,0:T(8,128)(2,1)S(1)} %fusion.2.refs_0_), channel_id=1, source_target_pairs={{0,4},{1,5},{2,6},{3,7},{4,0},{5,1},{6,2},{7,3},{8,12},{9,13},{10,... | collective-permute-start | bytes 2359304 | tf_op jit(solution)/shard_map/ppermute | solution.py:504
  18.9 28.9 %collective-permute-start = (bf16[192,2048]{1,0:T(8,128)(2,1)S(1)}, bf16[192,2048]{1,0:T(8,128)(2,1)}, u32[]{:S(2)}, u32[]{:S(2)}) collective-permute-start(bf16[192,2048]{1,0:T(8,128)(2,1)S(1)} %fusion.2.refs_0_), channel_id=1, source_target_pairs={{0,1},{1,0},{2,3},{3,2},{4,5},{5,4},{6,7},{7,6},{8,9},{9,8},{10,11... | collective-permute-start | bytes 2359304 | tf_op jit(solution)/shard_map/ppermute | solution.py:504
  19.8 25.8 %collective-permute-start.32 = (bf16[512,512]{1,0:T(8,128)(2,1)}, bf16[512,512]{1,0:T(8,128)(2,1)}, u32[]{:S(2)}, u32[]{:S(2)}) collective-permute-start(bf16[512,512]{1,0:T(8,128)(2,1)} %pad_maximum_fusion.3.refs_0_), channel_id=1, source_target_pairs={{0,8},{1,9},{2,10},{3,11},{4,12},{5,13},{6,14},{7,15},{8,0},{9,1},... | collective-permute-start | bytes 1572872 | tf_op jit(solution)/shard_map/ppermute | solution.py:504
  23.5 24.2 %collective-permute-start.33 = (bf16[512,512]{1,0:T(8,128)(2,1)}, bf16[512,512]{1,0:T(8,128)(2,1)}, u32[]{:S(2)}, u32[]{:S(2)}) collective-permute-start(bf16[512,512]{1,0:T(8,128)(2,1)} %pad_maximum_fusion.3.refs_0_), channel_id=1, source_target_pairs={{8,16},{9,17},{10,18},{11,19},{12,20},{13,21},{14,22},{15,23},{16,... | collective-permute-start | bytes 1572872 | tf_op jit(solution)/shard_map/ppermute | solution.py:504
  25.0 15.1 %collective-permute-start.12 = (bf16[512,256]{1,0:T(8,128)(2,1)}, bf16[512,256]{1,0:T(8,128)(2,1)}, u32[]{:S(2)}, u32[]{:S(2)}) collective-permute-start(bf16[512,256]{1,0:T(8,128)(2,1)} %collective-permute-done.11.refs_12_), channel_id=1, source_target_pairs={{8,0},{9,1},{10,2},{11,3},{12,4},{13,5},{14,6},{15,7},{16,24},{17,... | collective-permute-start | bytes 786440 | tf_op jit(solution)/shard_map/ppermute | solution.py:504
  47.8 11.1 %collective-permute-start.2 = (bf16[192,2048]{1,0:T(8,128)(2,1)S(1)}, bf16[192,2048]{1,0:T(8,128)(2,1)}, u32[]{:S(2)}, u32[]{:S(2)}) collective-permute-start(bf16[192,2048]{1,0:T(8,128)(2,1)S(1)} %collective-permute-done.1.refs_2_), channel_id=1, source_target_pairs={{0,1},{1,0},{2,3},{3,2},{4,5},{5,4},{6,7},{7,6},{8,9},{9,8},{10,11... | collective-permute-start | bytes 2359304 | tf_op jit(solution)/shard_map/ppermute | solution.py:504
  47.8 12.6 %collective-permute-start.4 = (bf16[192,2048]{1,0:T(8,128)(2,1)S(1)}, bf16[192,2048]{1,0:T(8,128)(2,1)}, u32[]{:S(2)}, u32[]{:S(2)}) collective-permute-start(bf16[192,2048]{1,0:T(8,128)(2,1)S(1)} %collective-permute-done.3.refs_4_), channel_id=1, source_target_pairs={{0,1},{1,0},{2,3},{3,2},{4,5},{5,4},{6,7},{7,6},{8,9},{9,8},{10,11... | collective-permute-start | bytes 2359304 | tf_op jit(solution)/shard_map/ppermute | solution.py:504
  55.7 32.4 %collective-permute-start.34 = (bf16[512,512]{1,0:T(8,128)(2,1)}, bf16[512,512]{1,0:T(8,128)(2,1)S(1)}, u32[]{:S(2)}, u32[]{:S(2)}) collective-permute-start(bf16[512,512]{1,0:T(8,128)(2,1)} %collective-permute-done.33.refs_2_), channel_id=1, source_target_pairs={{8,0},{9,1},{10,2},{11,3},{12,4},{13,5},{14,6},{15,7},{16,24},{17,... | collective-permute-start | bytes 1572872 | tf_op jit(solution)/shard_map/ppermute | solution.py:504
  57.0 41.4 %collective-permute-start.36 = (bf16[512,512]{1,0:T(8,128)(2,1)}, bf16[512,512]{1,0:T(8,128)(2,1)S(1)}, u32[]{:S(2)}, u32[]{:S(2)}) collective-permute-start(bf16[512,512]{1,0:T(8,128)(2,1)} %collective-permute-done.35.refs_4_), channel_id=1, source_target_pairs={{8,0},{9,1},{10,2},{11,3},{12,4},{13,5},{14,6},{15,7},{16,24},{17,... | collective-permute-start | bytes 1572872 | tf_op jit(solution)/shard_map/ppermute | solution.py:504
  58.4 46.0 %collective-permute-start.37 = (bf16[768,128]{1,0:T(8,128)(2,1)}, bf16[768,128]{1,0:T(8,128)(2,1)S(1)}, u32[]{:S(2)}, u32[]{:S(2)}) collective-permute-start(bf16[768,128]{1,0:T(8,128)(2,1)} %dynamic-slice_convert_fusion), channel_id=1, source_target_pairs={{0,4},{1,5},{2,6},{3,7},{4,0},{5,1},{6,2},{7,3},{8,12},{9,13},{10,... | collective-permute-start | bytes 589832 | tf_op jit(solution)/shard_map/ppermute | solution.py:504
  58.9 51.1 %collective-permute-start.21 = (bf16[256,512]{1,0:T(8,128)(2,1)}, bf16[256,512]{1,0:T(8,128)(2,1)S(1)}, u32[]{:S(2)}, u32[]{:S(2)}) collective-permute-start(bf16[256,512]{1,0:T(8,128)(2,1)} %pad_maximum_fusion.5), channel_id=1, source_target_pairs={{0,4},{1,5},{2,6},{3,7},{4,0},{5,1},{6,2},{7,3},{8,12},{9,13},{10,... | collective-permute-start | bytes 786440 | tf_op jit(solution)/shard_map/ppermute | solution.py:504
  69.4 16.2 %collective-permute-start.15 = (bf16[32,128]{1,0:T(8,128)(2,1)S(1)}, bf16[32,128]{1,0:T(8,128)(2,1)S(1)}, u32[]{:S(2)}, u32[]{:S(2)}) collective-permute-start(bf16[32,128]{1,0:T(8,128)(2,1)S(1)} %slice.11), channel_id=1, source_target_pairs={{0,8},{1,9},{2,10},{3,11},{4,12},{5,13},{6,14},{7,15},{8,16},{9,17... | collective-permute-start | bytes 24584 | tf_op jit(solution)/shard_map/ppermute | solution.py:504
  85.6 25.8 %collective-permute-start.27 = (bf16[256,512]{1,0:T(8,128)(2,1)S(1)}, bf16[256,512]{1,0:T(8,128)(2,1)S(1)}, u32[]{:S(2)}, u32[]{:S(2)}) collective-permute-start(bf16[256,512]{1,0:T(8,128)(2,1)S(1)} %pad_maximum_fusion.6), channel_id=1, source_target_pairs={{0,0},{1,8},{2,16},{3,24},{4,4},{5,12},{6,20},{7,28},{8,1},{9,9},{... | collective-permute-start | bytes 786440 | tf_op jit(solution)/shard_map/ppermute | solution.py:504
  88.1 35.4 %collective-permute-start.16 = (bf16[1552,128]{1,0:T(8,128)(2,1)S(1)}, bf16[1552,128]{1,0:T(8,128)(2,1)S(1)}, u32[]{:S(2)}, u32[]{:S(2)}) collective-permute-start(bf16[1552,128]{1,0:T(8,128)(2,1)S(1)} %shard_map.181.refs_0_), channel_id=1, source_target_pairs={{0,2},{1,3},{2,0},{3,1},{4,6},{5,7},{6,4},{7,5},{8,10},{9,11},{10,... | collective-permute-start | bytes 1191944 | tf_op jit(solution)/shard_map/ppermute | solution.py:504
  98.4 25.7 %collective-permute-start.17 = (bf16[1552,128]{1,0:T(8,128)(2,1)S(1)}, bf16[1552,128]{1,0:T(8,128)(2,1)S(1)}, u32[]{:S(2)}, u32[]{:S(2)}) collective-permute-start(bf16[1552,128]{1,0:T(8,128)(2,1)S(1)} %shard_map.181.refs_0_), channel_id=1, source_target_pairs={{0,4},{1,5},{2,6},{3,7},{4,0},{5,1},{6,2},{7,3},{8,12},{9,13},{10,... | collective-permute-start | bytes 1191944 | tf_op jit(solution)/shard_map/ppermute | solution.py:504
  104.4 20.2 %collective-permute-start.18 = (bf16[1552,128]{1,0:T(8,128)(2,1)S(1)}, bf16[1552,128]{1,0:T(8,128)(2,1)S(1)}, u32[]{:S(2)}, u32[]{:S(2)}) collective-permute-start(bf16[1552,128]{1,0:T(8,128)(2,1)S(1)} %shard_map.181.refs_0_), channel_id=1, source_target_pairs={{0,6},{1,7},{2,4},{3,5},{4,2},{5,3},{6,0},{7,1},{8,14},{9,15},{10,... | collective-permute-start | bytes 1191944 | tf_op jit(solution)/shard_map/ppermute | solution.py:504
  120.3 25.8 %collective-permute-start.22 = (bf16[512,512]{1,0:T(8,128)(2,1)S(1)}, bf16[512,512]{1,0:T(8,128)(2,1)S(1)}, u32[]{:S(2)}, u32[]{:S(2)}) collective-permute-start(bf16[512,512]{1,0:T(8,128)(2,1)S(1)} %pad_maximum_fusion.2.refs_0_), channel_id=1, source_target_pairs={{0,8},{1,9},{2,10},{3,11},{4,12},{5,13},{6,14},{7,15},{8,0},{9,1},... | collective-permute-start | bytes 1572872 | tf_op jit(solution)/shard_map/ppermute | solution.py:504
  122.1 23.3 %collective-permute-start.28 = (bf16[256,512]{1,0:T(8,128)(2,1)S(1)}, bf16[256,512]{1,0:T(8,128)(2,1)S(1)}, u32[]{:S(2)}, u32[]{:S(2)}) collective-permute-start(bf16[256,512]{1,0:T(8,128)(2,1)S(1)} %collective-permute-done.27.refs_6_), channel_id=1, source_target_pairs={{0,8},{1,9},{2,10},{3,11},{4,12},{5,13},{6,14},{7,15},{8,0},{9,1},... | collective-permute-start | bytes 786440 | tf_op jit(solution)/shard_map/ppermute | solution.py:504
  123.5 12.1 %collective-permute-start.41 = (bf16[1536,128]{1,0:T(8,128)(2,1)S(1)}, bf16[1536,128]{1,0:T(8,128)(2,1)S(1)}, u32[]{:S(2)}, u32[]{:S(2)}) collective-permute-start(bf16[1536,128]{1,0:T(8,128)(2,1)S(1)} %finish.1.refs_10_), channel_id=1, source_target_pairs={{0,2},{1,3},{2,0},{3,1},{4,6},{5,7},{6,4},{7,5},{8,10},{9,11},{10,... | collective-permute-start | bytes 1179656 | tf_op jit(solution)/shard_map/ppermute | solution.py:504
  124.1 17.3 %collective-permute-start.42 = (bf16[1536,128]{1,0:T(8,128)(2,1)S(1)}, bf16[1536,128]{1,0:T(8,128)(2,1)S(1)}, u32[]{:S(2)}, u32[]{:S(2)}) collective-permute-start(bf16[1536,128]{1,0:T(8,128)(2,1)S(1)} %finish.1.refs_10_), channel_id=1, source_target_pairs={{0,4},{1,5},{2,6},{3,7},{4,0},{5,1},{6,2},{7,3},{8,12},{9,13},{10,... | collective-permute-start | bytes 1179656 | tf_op jit(solution)/shard_map/ppermute | solution.py:504
  124.6 16.8 %collective-permute-start.43 = (bf16[1536,128]{1,0:T(8,128)(2,1)S(1)}, bf16[1536,128]{1,0:T(8,128)(2,1)S(1)}, u32[]{:S(2)}, u32[]{:S(2)}) collective-permute-start(bf16[1536,128]{1,0:T(8,128)(2,1)S(1)} %finish.1.refs_10_), channel_id=1, source_target_pairs={{0,6},{1,7},{2,4},{3,5},{4,2},{5,3},{6,0},{7,1},{8,14},{9,15},{10,... | collective-permute-start | bytes 1179656 | tf_op jit(solution)/shard_map/ppermute | solution.py:504
  135.6 25.4 %collective-permute-start.20 = (bf16[4656,128]{1,0:T(8,128)(2,1)S(1)}, bf16[4656,128]{1,0:T(8,128)(2,1)S(1)}, u32[]{:S(2)}, u32[]{:S(2)}) collective-permute-start(bf16[4656,128]{1,0:T(8,128)(2,1)S(1)} %pad_maximum_fusion), channel_id=1, source_target_pairs={{0,1},{1,0},{2,3},{3,2},{4,5},{5,4},{6,7},{7,6},{8,9},{9,8},{10,11... | collective-permute-start | bytes 3575816 | tf_op jit(solution)/shard_map/ppermute | solution.py:504
  141.5 58.1 %collective-permute-start.45 = (bf16[4608,128]{1,0:T(8,128)(2,1)S(1)}, bf16[4608,128]{1,0:T(8,128)(2,1)S(1)}, u32[]{:S(2)}, u32[]{:S(2)}) collective-permute-start(bf16[4608,128]{1,0:T(8,128)(2,1)S(1)} %pad_maximum_fusion.1), channel_id=1, source_target_pairs={{0,1},{1,0},{2,3},{3,2},{4,5},{5,4},{6,7},{7,6},{8,9},{9,8},{10,11... | collective-permute-start | bytes 3538952 | tf_op jit(solution)/shard_map/ppermute | solution.py:504
  141.6 16.0 %collective-permute-start.29 = (bf16[256,512]{1,0:T(8,128)(2,1)S(1)}, bf16[256,512]{1,0:T(8,128)(2,1)S(1)}, u32[]{:S(2)}, u32[]{:S(2)}) collective-permute-start(bf16[256,512]{1,0:T(8,128)(2,1)S(1)} %collective-permute-done.27.refs_6_), channel_id=1, source_target_pairs={{0,16},{1,17},{2,18},{3,19},{4,20},{5,21},{6,22},{7,23},{8,24},{9,... | collective-permute-start | bytes 786440 | tf_op jit(solution)/shard_map/ppermute | solution.py:504
  145.3 12.3 %collective-permute-start.23 = (bf16[512,512]{1,0:T(8,128)(2,1)S(1)}, bf16[512,512]{1,0:T(8,128)(2,1)S(1)}, u32[]{:S(2)}, u32[]{:S(2)}) collective-permute-start(bf16[512,512]{1,0:T(8,128)(2,1)S(1)} %pad_maximum_fusion.2.refs_0_), channel_id=1, source_target_pairs={{8,16},{9,17},{10,18},{11,19},{12,20},{13,21},{14,22},{15,23},{16,... | collective-permute-start | bytes 1572872 | tf_op jit(solution)/shard_map/ppermute | solution.py:504
  146.0 12.9 %collective-permute-start.25 = (bf16[512,512]{1,0:T(8,128)(2,1)S(1)}, bf16[512,512]{1,0:T(8,128)(2,1)S(1)}, u32[]{:S(2)}, u32[]{:S(2)}) collective-permute-start(bf16[512,512]{1,0:T(8,128)(2,1)S(1)} %collective-permute-done.22.refs_1_), channel_id=1, source_target_pairs={{8,16},{9,17},{10,18},{11,19},{12,20},{13,21},{14,22},{15,23},{16,... | collective-permute-start | bytes 1572872 | tf_op jit(solution)/shard_map/ppermute | solution.py:504
  157.7 30.8 %collective-permute-start.24 = (bf16[512,512]{1,0:T(8,128)(2,1)S(1)}, bf16[512,512]{1,0:T(8,128)(2,1)S(1)}, u32[]{:S(2)}, u32[]{:S(2)}) collective-permute-start(bf16[512,512]{1,0:T(8,128)(2,1)S(1)} %collective-permute-done.23.refs_2_), channel_id=1, source_target_pairs={{8,0},{9,1},{10,2},{11,3},{12,4},{13,5},{14,6},{15,7},{16,24},{17,... | collective-permute-start | bytes 1572872 | tf_op jit(solution)/shard_map/ppermute | solution.py:504
  159.0 40.7 %collective-permute-start.26 = (bf16[512,512]{1,0:T(8,128)(2,1)S(1)}, bf16[512,512]{1,0:T(8,128)(2,1)S(1)}, u32[]{:S(2)}, u32[]{:S(2)}) collective-permute-start(bf16[512,512]{1,0:T(8,128)(2,1)S(1)} %collective-permute-done.25.refs_4_), channel_id=1, source_target_pairs={{8,0},{9,1},{10,2},{11,3},{12,4},{13,5},{14,6},{15,7},{16,24},{17,... | collective-permute-start | bytes 1572872 | tf_op jit(solution)/shard_map/ppermute | solution.py:504
  160.5 39.2 %collective-permute-start.44 = (bf16[1536,128]{1,0:T(8,128)(2,1)S(1)}, bf16[1536,128]{1,0:T(8,128)(2,1)S(1)}, u32[]{:S(2)}, u32[]{:S(2)}) collective-permute-start(bf16[1536,128]{1,0:T(8,128)(2,1)S(1)} %finish.1.refs_10_), channel_id=1, source_target_pairs={{0,1},{1,0},{2,3},{3,2},{4,5},{5,4},{6,7},{7,6},{8,9},{9,8},{10,11... | collective-permute-start | bytes 1179656 | tf_op jit(solution)/shard_map/ppermute | solution.py:504
  161.0 10.2 %collective-permute-start.30 = (bf16[256,512]{1,0:T(8,128)(2,1)S(1)}, bf16[256,512]{1,0:T(8,128)(2,1)S(1)}, u32[]{:S(2)}, u32[]{:S(2)}) collective-permute-start(bf16[256,512]{1,0:T(8,128)(2,1)S(1)} %collective-permute-done.27.refs_6_), channel_id=1, source_target_pairs={{0,24},{1,25},{2,26},{3,27},{4,28},{5,29},{6,30},{7,31},{8,16},{9,... | collective-permute-start | bytes 786440 | tf_op jit(solution)/shard_map/ppermute | solution.py:504
  205.6 10.6 %collective-permute-start.46 = (bf16[768,256]{1,0:T(8,128)(2,1)S(1)}, bf16[768,256]{1,0:T(8,128)(2,1)S(1)}, u32[]{:S(2)}, u32[]{:S(2)}) collective-permute-start(bf16[768,256]{1,0:T(8,128)(2,1)S(1)} %combine.2), channel_id=1, source_target_pairs={{0,4},{1,5},{2,6},{3,7},{4,0},{5,1},{6,2},{7,3},{8,12},{9,13},{10,... | collective-permute-start | bytes 1179656 | tf_op jit(solution)/shard_map/ppermute | solution.py:504
  (33 other events, 348.1 us)
